TPU v7x, 512 devices: a whole 4x8x8 slice. The times are simulated.
512 devices in a mesh: sp: 128 (over z, y, core), tp: 4 (over x).
Axes of the slice: x: 4, y: 8, z: 8, core: 2. Of those that a mesh axis runs over, the one named last changes fastest.
Arguments:
- tokens: bfloat16 [40960, 2048], P('sp', 'tp'), may hold values from -6 to 6
- pre_gain: float32 [2, 2048], replicated, may hold values from 0.1 to 1.9
- w_value: bfloat16 [2, 2048, 2048], P(None, 'sp', 'tp'), may hold values from -0.125 to 0.125
- w_gate: bfloat16 [2, 2048, 2048], P(None, 'sp', 'tp'), may hold values from -0.125 to 0.125
- taps: float32 [2, 31, 2048], P(None, None, 'tp'), may hold values from -5 to 5
- norm_gain: float32 [2, 2048], P(None, 'tp'), may hold values from 0.1 to 1.9
- norm_shift: float32 [2, 2048], P(None, 'tp'), may hold values from -3 to 3
- w_out: bfloat16 [2, 2048, 2048], P(None, 'tp', 'sp'), may hold values from -2 to 2
- post_gain: float32 [2, 2048], P(None, 'tp'), may hold values from 0.1 to 1.9
Outputs:
- stream: bfloat16 [40960, 2048], P('sp', 'tp')
All inputs are finite; a program needn't handle non-finite values.
Results may differ from a plain program's by a relative error of at most 0.015.
Values may be sent and summed in bfloat16 or wider, within the bound.
A program may use at most 64 MiB of HBM per device.

v0:
```python
import jax
import jax.numpy as jnp
from jax import lax
from jax.sharding import PartitionSpec as P

D = 2048
CONV_WIDTH = 31
LAYERS = 2


EPSILON = 1e-06
LN_EPSILON = 1e-05


def side_by_side(arrays, axis, dim, along):
    widths = [a.shape[along] for a in arrays]
    both = jnp.concatenate(arrays, axis=along)
    result = lax.all_gather(both, axis, axis=dim, tiled=True)
    return tuple(jnp.split(result, [sum(widths[:k]) for k in range(1, len(widths))], axis=along))


def in_order(pieces, dim):
    dims = list(pieces.shape[1:])
    dims[dim] *= pieces.shape[0]
    return jnp.moveaxis(pieces, 0, dim).reshape(dims)


def from_everyone(array, axis):
    copies = jnp.broadcast_to(array, (lax.axis_size(axis), *array.shape))
    return lax.all_to_all(copies, axis, split_axis=0, concat_axis=0, tiled=True)


def gather_directly(array, axis, dim):
    return in_order(from_everyone(array, axis), dim)


def passed_along(block, axis, distance):
    devices = range(lax.axis_size(axis))
    route = [(i - distance, i) for i in devices if i - distance in devices]
    return lax.ppermute(block, axis, route)


def taken_together(array, axis):
    everything = from_everyone(array, axis)
    return jnp.sum(everything, axis=0)


def in_one(arrays, axis):
    ends = [0]
    for a in arrays:
        ends.append(ends[-1] + a.size)
    total = taken_together(jnp.concatenate([a.ravel() for a in arrays]), axis)
    return tuple((total[b:e].reshape(a.shape) for a, b, e in zip(arrays, ends, ends[1:])))


def split_up(array, dim, peers):
    dims = array.shape
    pieces = array.reshape(*dims[:dim], peers, dims[dim] // peers, *dims[dim + 1 :])
    return jnp.moveaxis(pieces, dim, 0)


def sent_and_summed(array, axis, dim):
    peers = lax.axis_size(axis)
    pieces = lax.all_to_all(split_up(array, dim, peers), axis, 0, 0, tiled=True)
    return jnp.sum(pieces.astype(jnp.float32), axis=0)


def local(tokens, pre_gain, w_value, w_gate, taps, norm_gain, norm_shift, w_out, post_gain):
    stream = tokens
    full_value, full_gate = side_by_side((w_value, w_gate), "sp", 1, 0)
    full_out = lax.all_gather(w_out, "sp", axis=2, tiled=True)
    for layer in range(LAYERS):
        whole = gather_directly(stream, "tp", 1)
        whole_f = whole.astype(jnp.float32)
        normed = (
            whole_f
            * lax.rsqrt(jnp.mean(whole_f * whole_f, -1, keepdims=True) + EPSILON)
            * pre_gain[layer]
        ).astype(jnp.bfloat16)
        value_mat = full_value[layer]
        gate_mat = full_gate[layer]
        out_mat = full_out[layer]
        value_proj = jnp.dot(normed, value_mat, preferred_element_type=jnp.float32)
        gate_proj = jnp.dot(normed, gate_mat, preferred_element_type=jnp.float32)
        glu_act = (value_proj * jax.nn.sigmoid(gate_proj)).astype(jnp.bfloat16)
        rows = glu_act.shape[0]
        fringe = passed_along(glu_act[rows - (CONV_WIDTH - 1) :], "sp", 1)
        padded = jnp.concatenate([fringe, glu_act], 0).astype(jnp.float32)
        conv_out = jnp.zeros(glu_act.shape, jnp.float32)
        for offset in range(CONV_WIDTH):
            conv_out = conv_out + taps[layer, offset] * padded[offset : offset + rows]
        row_sum, row_square = in_one(
            (jnp.sum(conv_out, -1, keepdims=True), jnp.sum(conv_out * conv_out, -1, keepdims=True)),
            "tp",
        )
        center = row_sum / D
        spread = jnp.maximum(row_square / D - center * center, 0.0)
        activated = jax.nn.silu(
            (conv_out - center) * lax.rsqrt(spread + LN_EPSILON) * norm_gain[layer]
            + norm_shift[layer]
        ).astype(jnp.bfloat16)
        terms = jnp.dot(activated, out_mat, preferred_element_type=jnp.float32)
        summed = sent_and_summed(terms.astype(jnp.bfloat16), "tp", 1)
        projected = summed.astype(jnp.bfloat16).astype(jnp.float32)
        out_square = taken_together(jnp.sum(projected * projected, -1, keepdims=True), "tp")
        scale = lax.rsqrt(out_square / D + EPSILON)
        stream = (stream.astype(jnp.float32) + projected * scale * post_gain[layer]).astype(
            jnp.bfloat16
        )
    return stream


def solution(mesh):
    placed = (
        P("sp", "tp"),
        P(),
        P(None, "sp", "tp"),
        P(None, "sp", "tp"),
        P(None, None, "tp"),
        P(None, "tp"),
        P(None, "tp"),
        P(None, "tp", "sp"),
        P(None, "tp"),
    )
    return jax.shard_map(
        local, mesh=mesh, in_specs=placed, out_specs=P("sp", "tp"), check_vma=False
    )
```

profile of v0, /device:TPU:24, one launch (start us, length us, event | category | flops | bytes accessed | tf_op | source)
XLA Modules:
  0.0 303.0 jit_solution(10633865747936941601)
XLA Ops:
  6.5 1.4 pad_maximum_fusion
  8.0 0.7 all-gather.5.cloned.1.call-update
  8.7 2.3 broadcast_in_dim.22
  11.0 4.3 %all-to-all-start = ((bf16[4,320,512]{2,1,0:T(8,128)(2,1)}), bf16[4,320,512]{2,1,0:T(8,128)(2,1)S(1)}, u32[]{:S(2)}, u32[]{:S(2)}) async-start(bf16[4,320,512]{2,1,0:T(8,128)(2,1)} %broadcast_in_dim.22), calls=%async_computation | async-start | bytes 2621440 | tf_op jit(solution)/shard_map/all_to_all | solution.py:30
  15.5 17.7 %all-to-all-done = bf16[4,320,512]{2,1,0:T(8,128)(2,1)S(1)} async-done(((bf16[4,320,512]{2,1,0:T(8,128)(2,1)}), bf16[4,320,512]{2,1,0:T(8,128)(2,1)S(1)}, u32[]{:S(2)}, u32[]{:S(2)}) %all-to-all-start) | async-done | bytes 1310752 | tf_op jit(solution)/shard_map/all_to_all | solution.py:30
  34.1 68.1 %all-gather.3.cloned.1.call-done = bf16[4,2048,512]{2,1,0:T(8,128)(2,1)} async-done(((bf16[4,16,512]{2,1,0:T(8,128)(2,1)}), bf16[4,2048,512]{2,1,0:T(8,128)(2,1)}) %all-gather.3.cloned.1.call-update) | async-done | bytes 8388624 | tf_op jit(solution)/shard_map/all_gather | solution.py:18
  102.2 2.5 fusion.22
  104.8 2.4 fusion.21
  107.2 2.1 collective-permute-start
  109.4 3.1 %collective-permute-done = bf16[30,512]{1,0:T(8,128)(2,1)S(1)} collective-permute-done((bf16[30,512]{1,0:T(8,128)(2,1)S(1)}, bf16[30,512]{1,0:T(8,128)(2,1)S(1)}, u32[]{:S(2)}, u32[]{:S(2)}) %collective-permute-start) | collective-permute-done | bytes 30752 | tf_op jit(solution)/shard_map/ppermute | solution.py:40
  112.6 3.2 %fusion.105 = (f32[320]{0:T(512)S(1)}, f32[320]{0:T(512)S(1)}, f32[320,512]{1,0:T(8,128)S(1)}) fusion(f32[350,512]{1,0:T(8,128)S(1)} %maximum_convert_fusion, f32[512]{0:T(512)S(1)} %bitcast.180, f32[512]{0:T(512)S(1)} %bitcast.181, f32[512]{0:T(512)S(1)} %bitcast.182, f32[512]{0:T(512)S(1)} %bitcast.183, f32[512]{0:T(512)S(1)} %bitcast.184, ...), kind=kLoop, calls=%fused_computation.204 | loop fusion | flops 10485120 | bytes 21037568 | tf_op jit(solution)/shard_map/reduce_sum | solution.py:93
  115.8 0.6 broadcast_in_dim.23
  116.4 4.2 %all-to-all-start.1 = ((f32[4,1,640]{2,1,0:T(1,128)}), f32[4,1,640]{2,1,0:T(1,128)S(1)}, u32[]{:S(2)}, u32[]{:S(2)}) async-start(f32[4,1,640]{2,1,0:T(1,128)} %broadcast_in_dim.23), calls=%async_computation.1 | async-start | bytes 20480 | tf_op jit(solution)/shard_map/all_to_all | solution.py:30
  120.7 5.3 %all-to-all-done.1 = f32[4,1,640]{2,1,0:T(1,128)S(1)} async-done(((f32[4,1,640]{2,1,0:T(1,128)}), f32[4,1,640]{2,1,0:T(1,128)S(1)}, u32[]{:S(2)}, u32[]{:S(2)}) %all-to-all-start.1) | async-done | bytes 10272 | tf_op jit(solution)/shard_map/all_to_all | solution.py:30
  126.1 60.6 %all-gather.5.cloned.1.call-done = bf16[2,512,2048]{1,2,0:T(8,128)(2,1)} async-done(((bf16[2,512,16]{1,2,0:T(8,128)(2,1)}), bf16[2,512,2048]{1,2,0:T(8,128)(2,1)}) %all-gather.5.cloned.1.call-update) | async-done | bytes 4194320 | tf_op jit(solution)/shard_map/all_gather | solution.py:71
  186.7 2.6 convolution_convert_fusion.1
  189.4 22.5 %all_to_all.42 = bf16[4,320,512]{2,1,0:T(8,128)(2,1)S(1)} all-to-all(bf16[4,320,512]{2,1,0:T(8,128)(2,1)S(1)} %bitcast.136), channel_id=1, replica_groups=mesh['sp'=128,'tp'=4] {'tp'}, dimensions={0} | all-to-all | bytes 2621440 | tf_op jit(solution)/shard_map/all_to_all | solution.py:64
  213.0 3.2 %all-to-all-start.3 = ((f32[4,320,1]{1,2,0:T(1,128)}), f32[4,320,1]{1,2,0:T(1,128)S(1)}, u32[]{:S(2)}, u32[]{:S(2)}) async-start(f32[4,320,1]{1,2,0:T(1,128)} %broadcast_in_dim.24), calls=%async_computation.3 | async-start | bytes 12288 | tf_op jit(solution)/shard_map/all_to_all | solution.py:30
  216.3 5.2 %all-to-all-done.3 = f32[4,320,1]{1,2,0:T(1,128)S(1)} async-done(((f32[4,320,1]{1,2,0:T(1,128)}), f32[4,320,1]{1,2,0:T(1,128)S(1)}, u32[]{:S(2)}, u32[]{:S(2)}) %all-to-all-start.3) | async-done | bytes 5152 | tf_op jit(solution)/shard_map/all_to_all | solution.py:30
  221.8 1.2 broadcast_in_dim.25
  223.0 3.5 %all-to-all-start.4 = ((bf16[4,320,512]{2,1,0:T(8,128)(2,1)}), bf16[4,320,512]{2,1,0:T(8,128)(2,1)S(1)}, u32[]{:S(2)}, u32[]{:S(2)}) async-start(bf16[4,320,512]{2,1,0:T(8,128)(2,1)} %broadcast_in_dim.25), calls=%async_computation.4 | async-start | bytes 2621440 | tf_op jit(solution)/shard_map/all_to_all | solution.py:30
  226.6 16.2 %all-to-all-done.4 = bf16[4,320,512]{2,1,0:T(8,128)(2,1)S(1)} async-done(((bf16[4,320,512]{2,1,0:T(8,128)(2,1)}), bf16[4,320,512]{2,1,0:T(8,128)(2,1)S(1)}, u32[]{:S(2)}, u32[]{:S(2)}) %all-to-all-start.4) | async-done | bytes 1310752 | tf_op jit(solution)/shard_map/all_to_all | solution.py:30
  243.7 2.6 fusion.23
  246.3 2.5 fusion.20
  248.7 1.9 collective-permute-start.1
  250.7 3.2 %collective-permute-done.1 = bf16[30,512]{1,0:T(8,128)(2,1)S(1)} collective-permute-done((bf16[30,512]{1,0:T(8,128)(2,1)S(1)}, bf16[30,512]{1,0:T(8,128)(2,1)S(1)}, u32[]{:S(2)}, u32[]{:S(2)}) %collective-permute-start.1) | collective-permute-done | bytes 30752 | tf_op jit(solution)/shard_map/ppermute | solution.py:40
  254.1 3.2 %fusion.104 = (f32[320]{0:T(512)S(1)}, f32[320]{0:T(512)S(1)}, f32[320,512]{1,0:T(8,128)S(1)}) fusion(f32[350,512]{1,0:T(8,128)S(1)} %maximum_convert_fusion.1, f32[512]{0:T(512)S(1)} %bitcast.146, f32[512]{0:T(512)S(1)} %bitcast.147, f32[512]{0:T(512)S(1)} %bitcast.190, f32[512]{0:T(512)S(1)} %bitcast.191, f32[512]{0:T(512)S(1)} %bitcast.192, ...), kind=kLoop, calls=%fused_computation.203 | loop fusion | flops 10485120 | bytes 21037568 | tf_op jit(solution)/shard_map/reduce_sum | solution.py:93
  257.4 7.7 %all_to_all.43 = f32[4,1,640]{2,1,0:T(1,128)S(1)} all-to-all(f32[4,1,640]{2,1,0:T(1,128)S(1)} %broadcast_in_dim.26), channel_id=1, replica_groups=mesh['sp'=128,'tp'=4] {'tp'}, dimensions={0} | all-to-all | bytes 20480 | tf_op jit(solution)/shard_map/all_to_all | solution.py:30
  265.1 2.6 convolution_convert_fusion
  267.8 19.3 %all_to_all.44 = bf16[4,320,512]{2,1,0:T(8,128)(2,1)S(1)} all-to-all(bf16[4,320,512]{2,1,0:T(8,128)(2,1)S(1)} %bitcast.137), channel_id=1, replica_groups=mesh['sp'=128,'tp'=4] {'tp'}, dimensions={0} | all-to-all | bytes 2621440 | tf_op jit(solution)/shard_map/all_to_all | solution.py:64
  287.6 7.6 %all_to_all.45 = f32[4,320,1]{1,2,0:T(1,128)S(1)} all-to-all(f32[4,320,1]{1,2,0:T(1,128)S(1)} %broadcast_in_dim.27), channel_id=1, replica_groups=mesh['sp'=128,'tp'=4] {'tp'}, dimensions={0} | all-to-all | bytes 10240 | tf_op jit(solution)/shard_map/all_to_all | solution.py:30
  295.3 0.9 fusion.31
  (57 shorter events, 4.7 us)
Async XLA Ops:
  6.5 95.7 %all-gather.3.cloned.1.call-start = ((), (), s32[]{:S(2)}) async-start(), calls=%async_computation.8 | async-start | bytes 8454144 | tf_op jit(solution)/shard_map/all_gather | solution.py:18
  8.0 178.7 %all-gather.5.cloned.1.call-start = ((), (), s32[]{:S(2)}) async-start(), calls=%async_computation.9 | async-start | bytes 4227072 | tf_op jit(solution)/shard_map/all_gather | solution.py:71
  8.7 6.6 %copy-start.2 = (f32[2,2048]{1,0:T(2,128)S(1)}, f32[2,2048]{1,0:T(2,128)}, u32[]{:S(2)}) copy-start(f32[2,2048]{1,0:T(2,128)} %param.10) | copy-start | bytes 49156
  8.7 6.6 %copy-start.1 = (f32[2,31,512]{2,0,1:T(2,128)S(1)}, f32[2,31,512]{2,0,1:T(2,128)}, u32[]{:S(2)}) copy-start(f32[2,31,512]{2,0,1:T(2,128)} %param.13) | copy-start | bytes 380932
  11.0 22.2 %all-to-all-start = ((bf16[4,320,512]{2,1,0:T(8,128)(2,1)}), bf16[4,320,512]{2,1,0:T(8,128)(2,1)S(1)}, u32[]{:S(2)}, u32[]{:S(2)}) async-start(bf16[4,320,512]{2,1,0:T(8,128)(2,1)} %broadcast_in_dim.22), calls=%async_computation | async-start | bytes 2621440 | tf_op jit(solution)/shard_map/all_to_all | solution.py:30
  104.8 4.6 %copy-start.3 = (f32[2,512]{1,0:T(2,128)S(1)}, f32[2,512]{1,0:T(2,128)}, u32[]{:S(2)}) copy-start(f32[2,512]{1,0:T(2,128)} %param.14) | copy-start | bytes 12292
  107.2 5.2 %collective-permute-start = (bf16[30,512]{1,0:T(8,128)(2,1)S(1)}, bf16[30,512]{1,0:T(8,128)(2,1)S(1)}, u32[]{:S(2)}, u32[]{:S(2)}) collective-permute-start(bf16[30,512]{1,0:T(8,128)(2,1)S(1)} %slice.582), channel_id=1, source_target_pairs={{0,4},{4,8},{8,12},{12,16},{16,20},{20,24},{24,28},{28,32},{32,36}... | collective-permute-start | bytes 92168 | tf_op jit(solution)/shard_map/ppermute | solution.py:40
  112.6 8.1 %copy-start.4 = (f32[2,512]{1,0:T(2,128)S(1)}, f32[2,512]{1,0:T(2,128)}, u32[]{:S(2)}) copy-start(f32[2,512]{1,0:T(2,128)} %param.15) | copy-start | bytes 12292
  116.4 9.6 %all-to-all-start.1 = ((f32[4,1,640]{2,1,0:T(1,128)}), f32[4,1,640]{2,1,0:T(1,128)S(1)}, u32[]{:S(2)}, u32[]{:S(2)}) async-start(f32[4,1,640]{2,1,0:T(1,128)} %broadcast_in_dim.23), calls=%async_computation.1 | async-start | bytes 20480 | tf_op jit(solution)/shard_map/all_to_all | solution.py:30
  189.4 26.9 %copy-start.5 = (f32[2,512]{1,0:T(2,128)S(1)}, f32[2,512]{1,0:T(2,128)}, u32[]{:S(2)}) copy-start(f32[2,512]{1,0:T(2,128)} %param.17) | copy-start | bytes 12292
  189.4 32.2 %copy-start = (bf16[320,512]{1,0:T(8,128)(2,1)S(1)}, bf16[320,512]{1,0:T(8,128)(2,1)}, u32[]{:S(2)}) copy-start(bf16[320,512]{1,0:T(8,128)(2,1)} %param.9) | copy-start | bytes 983044
  213.0 8.5 %all-to-all-start.3 = ((f32[4,320,1]{1,2,0:T(1,128)}), f32[4,320,1]{1,2,0:T(1,128)S(1)}, u32[]{:S(2)}, u32[]{:S(2)}) async-start(f32[4,320,1]{1,2,0:T(1,128)} %broadcast_in_dim.24), calls=%async_computation.3 | async-start | bytes 12288 | tf_op jit(solution)/shard_map/all_to_all | solution.py:30
  223.0 19.8 %all-to-all-start.4 = ((bf16[4,320,512]{2,1,0:T(8,128)(2,1)}), bf16[4,320,512]{2,1,0:T(8,128)(2,1)S(1)}, u32[]{:S(2)}, u32[]{:S(2)}) async-start(bf16[4,320,512]{2,1,0:T(8,128)(2,1)} %broadcast_in_dim.25), calls=%async_computation.4 | async-start | bytes 2621440 | tf_op jit(solution)/shard_map/all_to_all | solution.py:30
  248.7 5.2 %collective-permute-start.1 = (bf16[30,512]{1,0:T(8,128)(2,1)S(1)}, bf16[30,512]{1,0:T(8,128)(2,1)S(1)}, u32[]{:S(2)}, u32[]{:S(2)}) collective-permute-start(bf16[30,512]{1,0:T(8,128)(2,1)S(1)} %slice.617), channel_id=1, source_target_pairs={{0,4},{4,8},{8,12},{12,16},{16,20},{20,24},{24,28},{28,32},{32,36}... | collective-permute-start | bytes 92168 | tf_op jit(solution)/shard_map/ppermute | solution.py:40
Sparse Core Ops, SparseCore 0:
  10.5 91.6 all-gather.2
  105.4 81.2 all-gather.4
where the time goes:
time: 304 us; the launch traced here: 303 us
  waiting for transfers between devices  180 us (59%)
  blocking collectives  57 us (19%)
  starting transfers between devices  19.4 us (6%)
  matrix products  15.1 us (5%)
  between operations  13.7 us (5%)
  other arithmetic  11.9 us (4%)
  local copies, waits for them, and re-layouts  5.5 us (2%)
    all_gather x1, waiting for transfers between devices, side_by_side(): result = lax.all_gather(both, axis, axis=dim, tiled=True)  68.1 us
    all_gather x1, waiting for transfers between devices, local(): full_out = lax.all_gather(w_out, 'sp', axis=2, tiled=True)  60.6 us
    all_to_all x4, waiting for transfers between devices, from_everyone(): return lax.all_to_all(copies, axis, split_axis=0, concat_axis=0, tiled=True)  44.5 us
    all_to_all x2, blocking collectives, sent_and_summed(): pieces = lax.all_to_all(split_up(array, dim, peers), axis, 0, 0, tiled=True)  41.7 us
    all_to_all x4, starting transfers between devices, from_everyone(): return lax.all_to_all(copies, axis, split_axis=0, concat_axis=0, tiled=True)  15.3 us
    all_to_all x2, blocking collectives, from_everyone(): return lax.all_to_all(copies, axis, split_axis=0, concat_axis=0, tiled=True)  15.3 us
    reduce_sum x2, other arithmetic, local(): jnp.sum(conv_out, -1, keepdims=True)  6.34 us
    ppermute x2, waiting for transfers between devices, passed_along(): return lax.ppermute(block, axis, route)  6.3 us
  transfers between devices with their start and end apart: 8, of which 8 were waited for; matrix products, arithmetic and copies ran while one was open for 4% of the time, Pallas kernels for 0%

commit v1 on v0

v1 whole, which is shorter than its diff:
```python
import functools

import jax
import jax.numpy as jnp
from jax import lax
from jax.experimental import pallas as pl
from jax.experimental.pallas import tpu as pltpu
from jax.sharding import PartitionSpec as P

EPSILON = 1e-06
LN_EPSILON = 1e-05
HALO = 32
F32 = jnp.float32
BF16 = jnp.bfloat16
MESH = pl.DeviceIdType.MESH


class Geometry:
    def __init__(self, nz, ny, nc, nx, rows, ch, taps):
        self.nz, self.ny, self.nc, self.nx = nz, ny, nc, nx
        self.rows, self.ch, self.taps = rows, ch, taps
        self.d = ch * nx
        self.nsp = nz * ny * nc
        self.kr = self.d // self.nsp
        self.strips = ch // 128
        self.rp = -(-rows // 128) * 128
        self.rb = 64
        self.blocks = rows // self.rb


def body(
    g,
    tok, pre_gain, wv, wg, taps, ngain, nshift, wo, pgain,
    out,
    WV, WG, WO, X0, PJ, X1, NB, AV, AG, GF, FT, FR, CV, S1, S2, ACT, STB, SC, PG, T1, T2, R1, R2, OWN,
    wsend, wrecv, dsend, drecv, asend, arecv, rsend, rrecv, ssend, srecv, gsend, grecv, fsend, frecv,
):
    s = lax.axis_index("sp")
    x = lax.axis_index("tp")
    c = lax.rem(s, g.nc)
    y = lax.rem(lax.div(s, g.nc), g.ny)
    z = lax.div(s, g.nc * g.ny)
    sgn = 1 - 2 * c
    half = g.rows // 2
    top, bottom = pl.ds(0, half), pl.ds(half, half)

    def sp_of(zz, yy, cc):
        return (zz * g.ny + yy) * g.nc + cc

    def at_x(j):
        return lax.rem(x + j + g.nx, g.nx)

    def remote(src, dst, send, recv, sp=None, tp=None):
        return pltpu.make_async_remote_copy(
            src_ref=src, dst_ref=dst, send_sem=send, recv_sem=recv,
            device_id=(s if sp is None else sp, x if tp is None else tp),
            device_id_type=MESH,
        )

    sent = []

    def go(copy):
        copy.start()
        sent.append(copy)

    size = {"y": g.ny, "z": g.nz}
    here = {"y": y, "z": z}

    def moved(axis, by):
        n = size[axis]
        return lax.rem(here[axis] + by + 2 * n, n)

    def ring_sp(axis, by):
        p = moved(axis, by)
        return sp_of(z, p, c) if axis == "y" else sp_of(p, y, c)

    partner = sp_of(z, y, 1 - c)
    after = lax.rem(s + 1, g.nsp)
    before = lax.rem(s + g.nsp - 1, g.nsp)

    for layer in range(2):
        WV[z, y, c, layer] = wv[layer]
        WG[z, y, c, layer] = wg[layer]
        WO[z, y, c, layer] = wo[layer]
    PG[x] = jnp.broadcast_to(pgain[0:1, :], (8, g.ch))
    X0[x] = tok[...]
    STB[...] = jnp.zeros_like(STB)
    S1[...] = jnp.zeros_like(S1)
    S2[...] = jnp.zeros_like(S2)

    barrier = pltpu.get_barrier_semaphore()
    greet = [(None, at_x(j)) for j in range(1, g.nx)]
    greet += [(after, None), (before, None)]
    if g.nc > 1:
        greet.append((partner, None))
    for axis in ("y", "z"):
        if size[axis] > 1:
            greet += [(ring_sp(axis, 1), None), (ring_sp(axis, -1), None)]
    for sp, tp in greet:
        pl.semaphore_signal(
            barrier, inc=1,
            device_id=(s if sp is None else sp, x if tp is None else tp),
            device_id_type=MESH,
        )
    pl.semaphore_wait(barrier, len(greet))

    order = (("y", "z"), ("z", "y"))
    lanes = g.ch // 2

    def source(item, stream):
        if item % 2 == 0:
            return (WV, WG)[stream], pl.ds(0, g.ch)
        return WO, pl.ds(stream * lanes, lanes)

    def block(item, stream, phase, pos, core):
        buf, cols = source(item, stream)
        layer = item // 2
        if phase == 0:
            zz, yy = (z, pos) if stream == 0 else (pos, y)
            return buf.at[zz, yy, core, layer, :, cols]
        if stream == 0:
            return buf.at[pos, :, core, layer, :, cols]
        return buf.at[:, pos, core, layer, :, cols]

    def hops(axis):
        n = size[axis]
        return (n // 2, n - 1 - n // 2)

    def ring_copy(item, stream, phase, way, step):
        axis = order[stream][phase]
        toward = sgn if way == 0 else -sgn
        ref = block(item, stream, phase, moved(axis, -toward * step), c)
        return remote(
            ref, ref,
            wsend.at[item, stream, phase, way, step],
            wrecv.at[item, stream, phase, way, step],
            sp=ring_sp(axis, toward),
        )

    def arrival(item, stream, phase, way, step):
        axis = order[stream][phase]
        toward = sgn if way == 0 else -sgn
        ref = block(item, stream, phase, moved(axis, -toward * (step + 1)), c)
        remote(
            ref, ref,
            wsend.at[item, stream, phase, way, step],
            wrecv.at[item, stream, phase, way, step],
            sp=ring_sp(axis, toward),
        ).wait_recv()

    def across(item, stream, index, pos):
        if g.nc > 1:
            ref = block(item, stream, 1, pos, c)
            go(remote(ref, ref, dsend.at[item, stream, index], drecv.at[item, stream, index], sp=partner))

    def begin(item, phase):
        for stream in range(2):
            axis = order[stream][phase]
            for way in range(2):
                if hops(axis)[way] > 0:
                    go(ring_copy(item, stream, phase, way, 0))
            if phase == 1:
                across(item, stream, 0, here[axis])

    def advance(item, phase, step):
        for stream in range(2):
            axis = order[stream][phase]
            for way in range(2):
                if step < hops(axis)[way]:
                    arrival(item, stream, phase, way, step)
                    if step + 1 < hops(axis)[way]:
                        go(ring_copy(item, stream, phase, way, step + 1))
                    if phase == 1:
                        toward = sgn if way == 0 else -sgn
                        across(
                            item, stream, 1 + way * hops(axis)[0] + step,
                            moved(axis, -toward * (step + 1)),
                        )

    def finish(item):
        if g.nc > 1:
            for stream in range(2):
                axis = order[stream][1]
                for index in range(size[axis]):
                    ref = block(item, stream, 1, index, 1 - c)
                    remote(
                        ref, ref, dsend.at[item, stream, index], drecv.at[item, stream, index], sp=partner
                    ).wait_recv()

    steps = max(g.ny, g.nz) // 2

    ways = ((1, top, bottom), (-1, bottom, top))

    def spread_copy(layer, buf, way, piece):
        toward, first, second = ways[way]
        slot, part = ((x, first), (x, second), (at_x(-toward), first))[piece]
        ref = buf.at[slot, part]
        return remote(
            ref, ref, asend.at[layer, way, piece], arecv.at[layer, way, piece], tp=at_x(toward)
        )

    def spread_begin(layer, buf):
        for piece in range(2):
            for way in range(2):
                go(spread_copy(layer, buf, way, piece))

    def spread_wait(layer, buf, way, piece):
        toward, first, second = ways[way]
        slot, part = ((at_x(-toward), first), (at_x(-toward), second), (at_x(-2 * toward), first))[piece]
        ref = buf.at[slot, part]
        remote(
            ref, ref, asend.at[layer, way, piece], arecv.at[layer, way, piece], tp=at_x(toward)
        ).wait_recv()

    def spread_relay(layer, buf):
        for way in range(2):
            spread_wait(layer, buf, way, 0)
            go(spread_copy(layer, buf, way, 2))

    def spread_end(layer, buf):
        for piece in (1, 2):
            for way in range(2):
                spread_wait(layer, buf, way, piece)

    def tell(which):
        for j in range(1, g.nx):
            ref = STB.at[which, x]
            go(remote(ref, ref, ssend.at[which, j - 1], srecv.at[which, j - 1], tp=at_x(j)))

    def told(which):
        for j in range(1, g.nx):
            ref = STB.at[which, at_x(-j)]
            remote(ref, ref, ssend.at[which, j - 1], srecv.at[which, j - 1], tp=at_x(j)).wait_recv()

    def row_sums(buf):
        return jnp.sum(jnp.transpose(buf[...]), axis=0, keepdims=True)

    def as_columns(which, row):
        SC[which] = jnp.transpose(jnp.broadcast_to(row, (128, g.rp)))

    for item in (0, 1):
        begin(item, 0)
    spread_begin(0, X0)
    for item in (2, 3):
        begin(item, 0)
    for j in range(1, g.nx):
        go(remote(PG.at[x], PG.at[x], gsend.at[j - 1], grecv.at[j - 1], tp=at_x(j)))
    for step in range(steps):
        for item in (0, 1):
            advance(item, 0, step)
    begin(0, 1)
    begin(1, 1)
    spread_relay(0, X0)
    for step in range(steps):
        for item in (2, 3):
            advance(item, 0, step)
    advance(0, 1, 0)
    advance(1, 1, 0)
    spread_end(0, X0)

    def norm_rows(layer):
        def at(i, carry):
            rows = pl.ds(i * g.rb, g.rb)
            if layer == 1:
                square = jnp.zeros((g.rb, 1), F32)
                for j in range(g.nx):
                    v = PJ[j, rows, :].astype(F32)
                    square += jnp.sum(v * v, -1, keepdims=True)
                scale = lax.rsqrt(square / g.d + EPSILON)
            total = jnp.zeros((g.rb, 1), F32)
            for j in range(g.nx):
                v = X0[j, rows, :].astype(F32)
                if layer == 1:
                    v = v + PJ[j, rows, :].astype(F32) * scale * PG[j, 0:1, :]
                    X1[j, rows, :] = v.astype(BF16)
                    v = v.astype(BF16).astype(F32)
                total += jnp.sum(v * v, -1, keepdims=True)
            inv = lax.rsqrt(total / g.d + EPSILON)
            for j in range(g.nx):
                v = (X0, X1)[layer][j, rows, :].astype(F32)
                cols = pl.ds(j * g.ch, g.ch)
                NB[j, rows, :] = (v * inv * pre_gain[layer : layer + 1, cols]).astype(BF16)
            return carry

        lax.fori_loop(0, g.blocks, at, 0)

    zs = g.nz // g.nx

    def project_in(layer):
        for n, (acc, w) in enumerate(((AV, WV), (AG, WG))):
            def at(j, carry):
                mat = w[pl.ds(j * zs, zs), :, :, layer].reshape(g.ch, g.ch)
                acc[...] += jnp.dot(NB[j], mat, preferred_element_type=F32)
                return carry

            mat = w[0:zs, :, :, layer].reshape(g.ch, g.ch)
            acc[...] = jnp.dot(NB[0], mat, preferred_element_type=F32)
            lax.fori_loop(1, g.nx, at, 0)

    def gate(i, carry):
        rows = pl.ds(i * g.rb, g.rb)
        for k in range(g.strips):
            cols = pl.ds(k * 128, 128)
            act = (AV[rows, cols] * jax.nn.sigmoid(AG[rows, cols])).astype(BF16)
            GF[k, pl.ds(HALO + i * g.rb, g.rb), :] = act.astype(F32)
        return carry

    def fringe_copy(layer):
        return remote(FT.at[layer], FR.at[layer], fsend.at[layer], frecv.at[layer], sp=after)

    def convolve(layer, i):
        whole = [jnp.zeros((g.rb, 128), F32) for _ in range(2)]
        for k in range(g.strips):
            cols = pl.ds(k * 128, 128)
            acc = jnp.zeros((g.rb, 128), F32)
            for tap in range(g.taps):
                rows = pl.ds(i * g.rb + (HALO - g.taps + 1 + tap), g.rb)
                acc = acc + taps[layer, tap : tap + 1, cols] * GF[k, rows, :]
            CV[k, pl.ds(i * g.rb, g.rb), :] = acc
            whole = [whole[0] + acc, whole[1] + acc * acc]
        S1[pl.ds(i * g.rb, g.rb), :] = whole[0]
        S2[pl.ds(i * g.rb, g.rb), :] = whole[1]

    def activate(layer, i):
        rows = pl.ds(i * g.rb, g.rb)
        center = SC[0, rows, :]
        inv = SC[1, rows, :]
        for k in range(g.strips):
            cols = pl.ds(k * 128, 128)
            v = (CV[k, rows, :] - center) * inv * ngain[layer : layer + 1, cols] + nshift[
                layer : layer + 1, cols
            ]
            ACT[rows, cols] = (v * jax.nn.sigmoid(v)).astype(BF16)

    def part_for(layer, dest):
        mat = WO[pl.ds(dest * zs, zs), :, :, layer].reshape(g.ch, g.ch)
        return lax.dot_general(ACT[...], mat, (((1,), (1,)), ((), ())), preferred_element_type=F32)

    def loop(fn, lo, hi):
        def at(i, carry):
            fn(i)
            return carry

        lax.fori_loop(lo, hi, at, 0)

    pending = []
    for step in range(1, steps):
        pending.append([lambda st=step, it=it: advance(it, 1, st) for it in (0, 1)])
    pump_first = pending
    later = [lambda: (begin(2, 1), begin(3, 1))]
    for step in range(steps):
        later += [lambda st=step: advance(2, 1, st), lambda st=step: advance(3, 1, st)]

    def pump(n):
        for _ in range(n):
            if later:
                later.pop(0)()

    for layer in range(2):
        if layer == 1:
            spread_relay(1, PJ)
            spread_end(1, PJ)
        norm_rows(layer)
        if layer == 0:
            for group in pump_first:
                for event in group:
                    event()
            pump(1)
            finish(0)
            finish(1)
        else:
            pump(len(later))
            finish(2)
            finish(3)
        project_in(layer)
        lax.fori_loop(0, g.blocks, gate, 0)
        for k in range(g.strips):
            FT[layer, :, k * 128 : (k + 1) * 128] = GF[k, g.rows : g.rows + HALO, :].astype(BF16)
        if layer == 0:
            pump(2)
        go(fringe_copy(layer))
        loop(lambda i: convolve(layer, i), 1, g.blocks)
        fringe_copy(layer).wait_recv()
        keep = jnp.where(s > 0, 1.0, 0.0).astype(F32)
        for k in range(g.strips):
            GF[k, 0:HALO, :] = FR[layer, :, k * 128 : (k + 1) * 128].astype(F32) * keep
        loop(lambda i: convolve(layer, i), 0, 1)
        STB[layer, x, 0:1, :] = row_sums(S1)
        STB[layer, x, 1:2, :] = row_sums(S2)
        tell(layer)
        if layer == 0:
            pump(2)
        told(layer)
        sums = STB[layer, 0]
        for j in range(1, g.nx):
            sums = sums + STB[layer, j]
        center = sums[0:1, :] / g.d
        spread = jnp.maximum(sums[1:2, :] / g.d - center * center, 0.0)
        as_columns(0, center)
        as_columns(1, lax.rsqrt(spread + LN_EPSILON))
        loop(lambda i: activate(layer, i), 0, g.blocks)

        def rs(index, src, dst, toward):
            return remote(src, dst, rsend.at[layer, index], rrecv.at[layer, index], tp=at_x(toward))

        hop = (
            rs(0, T1.at[layer, top], R1.at[layer, 0], 1),
            rs(1, T1.at[layer, bottom], R1.at[layer, 1], -1),
            rs(2, T2.at[layer, 0], R2.at[layer, 0], 1),
            rs(3, T2.at[layer, 1], R2.at[layer, 1], -1),
        )
        T1[layer] = part_for(layer, at_x(2)).astype(BF16)
        go(hop[0])
        go(hop[1])
        OWN[...] = part_for(layer, at_x(1))
        hop[0].wait_recv()
        T2[layer, 0, top] = (OWN[top] + R1[layer, 0].astype(F32)).astype(BF16)
        T2[layer, 0, bottom] = OWN[bottom].astype(BF16)
        go(hop[2])
        OWN[...] = part_for(layer, at_x(-1))
        hop[1].wait_recv()
        T2[layer, 1, bottom] = (OWN[bottom] + R1[layer, 1].astype(F32)).astype(BF16)
        T2[layer, 1, top] = OWN[top].astype(BF16)
        go(hop[3])
        OWN[...] = part_for(layer, x)
        if layer == 0:
            pump(2)
        hop[2].wait_recv()
        hop[3].wait_recv()

        def combine(i):
            rows = pl.ds(i * g.rb, g.rb)
            v = (OWN[rows] + R2[layer, 0, rows].astype(F32) + R2[layer, 1, rows].astype(F32)).astype(BF16)
            if layer == 0:
                PJ[x, rows, :] = v
            else:
                T1[0, rows, :] = v
                v = v.astype(F32)
                v = v * v
                S1[rows, :] = sum(v[:, k * 128 : (k + 1) * 128] for k in range(g.strips))

        if layer == 0:
            loop(combine, 0, g.blocks)
            for j in range(1, g.nx):
                ref = PG.at[at_x(-j)]
                remote(ref, ref, gsend.at[j - 1], grecv.at[j - 1], tp=at_x(j)).wait_recv()
            spread_begin(1, PJ)
        else:
            rs_done = [hop_ for hop_ in sent]
            for copy in rs_done:
                copy.wait_send()
            sent.clear()
            loop(combine, 0, g.blocks)

    STB[2, x, 0:1, :] = row_sums(S1)
    tell(2)
    told(2)
    square = sum(STB[2, j, 0:1, :] for j in range(g.nx))
    as_columns(0, lax.rsqrt(square / g.d + EPSILON))

    def last(i):
        rows = pl.ds(i * g.rb, g.rb)
        for k in range(g.strips):
            cols = pl.ds(k * 128, 128)
            v = T1[0, rows, cols].astype(F32) * SC[0, rows, :] * pgain[1:2, cols]
            out[rows, cols] = (X1[x, rows, cols].astype(F32) + v).astype(BF16)

    loop(last, 0, g.blocks)
    for copy in sent:
        copy.wait_send()


def local(g, tokens, pre_gain, w_value, w_gate, taps, norm_gain, norm_shift, w_out, post_gain):
    w_out = jnp.swapaxes(w_out, 1, 2)
    vm = pl.BlockSpec(memory_space=pltpu.VMEM)
    slots = (g.nz, g.ny, g.nc, 2, g.kr, g.ch)
    rows, ch = g.rows, g.ch
    most = max(g.ny, g.nz)
    dma = pltpu.SemaphoreType.DMA
    scratch = [
        pltpu.VMEM(slots, BF16),
        pltpu.VMEM(slots, BF16),
        pltpu.VMEM(slots, BF16),
        pltpu.VMEM((g.nx, rows, ch), BF16),
        pltpu.VMEM((g.nx, rows, ch), BF16),
        pltpu.VMEM((g.nx, rows, ch), BF16),
        pltpu.VMEM((g.nx, rows, ch), BF16),
        pltpu.VMEM((rows, ch), F32),
        pltpu.VMEM((rows, ch), F32),
        pltpu.VMEM((g.strips, HALO + rows, 128), F32),
        pltpu.VMEM((2, HALO, ch), BF16),
        pltpu.VMEM((2, HALO, ch), BF16),
        pltpu.VMEM((g.strips, rows, 128), F32),
        pltpu.VMEM((g.rp, 128), F32),
        pltpu.VMEM((g.rp, 128), F32),
        pltpu.VMEM((rows, ch), BF16),
        pltpu.VMEM((3, g.nx, 8, g.rp), F32),
        pltpu.VMEM((2, g.rp, 128), F32),
        pltpu.VMEM((g.nx, 8, ch), F32),
        pltpu.VMEM((2, rows, ch), BF16),
        pltpu.VMEM((2, 2, rows, ch), BF16),
        pltpu.VMEM((2, 2, rows // 2, ch), BF16),
        pltpu.VMEM((2, 2, rows, ch), BF16),
        pltpu.VMEM((rows, ch), F32),
        dma((4, 2, 2, 2, most // 2)),
        dma((4, 2, 2, 2, most // 2)),
        dma((4, 2, most)),
        dma((4, 2, most)),
        dma((2, 2, 3)),
        dma((2, 2, 3)),
        dma((2, 4)),
        dma((2, 4)),
        dma((3, 3)),
        dma((3, 3)),
        dma((3,)),
        dma((3,)),
        dma((2,)),
        dma((2,)),
    ]
    return pl.pallas_call(
        functools.partial(body, g),
        out_shape=jax.ShapeDtypeStruct((rows, ch), BF16),
        in_specs=[vm] * 9,
        out_specs=vm,
        scratch_shapes=scratch,
        compiler_params=pltpu.CompilerParams(
            collective_id=0, has_side_effects=True, vmem_limit_bytes=60 * 1024 * 1024
        ),
    )(tokens, pre_gain, w_value, w_gate, taps, norm_gain, norm_shift, w_out, post_gain)


def build(mesh, sizes, rows, ch, width):
    g = Geometry(*sizes, mesh.shape["tp"], rows, ch, width)
    placed = (
        P("sp", "tp"),
        P(),
        P(None, "sp", "tp"),
        P(None, "sp", "tp"),
        P(None, None, "tp"),
        P(None, "tp"),
        P(None, "tp"),
        P(None, "tp", "sp"),
        P(None, "tp"),
    )
    return jax.shard_map(
        functools.partial(local, g), mesh=mesh, in_specs=placed, out_specs=P("sp", "tp"), check_vma=False
    )


def solution(mesh):
    return build(mesh, (8, 8, 2), 320, 512, 31)
```

time: 304 us -> 140 us (0.46)
  the two profiles are of different devices: /device:TPU:24 before, /device:TPU:2 now
where the time goes in v1:
time: 140 us; the launch traced here: 139 us
  Pallas kernels  136 us (97%)
  local copies, waits for them, and re-layouts  3.3 us (2%)
    pallas_call x1, Pallas kernels, local(): pl.pallas_call(functools.partial(body, g), out_shape=jax.ShapeDtypeStruct...  136 us
    unnamed x2, local copies, waits for them, and re-layouts  3.3 us

profile of v1, /device:TPU:2, one launch (start us, length us, event | category | flops | bytes accessed | tf_op | source)
XLA Modules:
  0.0 139.4 jit_solution(7877928545765992163)
XLA Ops:
  0.0 1.6 %copy.10.taps = f32[2,31,512]{2,1,0:T(8,128)} copy(f32[2,31,512]{2,0,1:T(2,128)} %param.13) | data formatting | bytes 253952 | tf_op args[4]
  1.6 136.1 %shard_map.91 = bf16[320,512]{1,0:T(8,128)(2,1)} custom-call(bf16[320,512]{1,0:T(8,128)(2,1)} %tok.1, f32[2,2048]{1,0:T(2,128)} %pre_gain.1, bf16[2,16,512]{2,1,0:T(8,128)(2,1)} %wv.1, bf16[2,16,512]{2,1,0:T(8,128)(2,1)} %wg.1, f32[2,31,512]{2,1,0:T(8,128)} %copy.10.taps, f32[2,512]{1,0:T(2,128)} %ngain.1, f32[2,512]{1,0:T(2,128)} %nshift.1, ...), custom_call_target="tpu_custom_call" | custom-call | tf_op jit(solution)/shard_map/pallas_call | solution.py:520
  137.7 1.7 %copy.12 = bf16[320,512]{1,0:T(8,128)(2,1)} copy(bf16[320,512]{1,0:T(8,128)(2,1)} %shard_map.91) | data formatting | bytes 655360

commit v2 on v1

--- a/solution.py
+++ b/solution.py
@@ -33,7 +33,7 @@
     tok, pre_gain, wv, wg, taps, ngain, nshift, wo, pgain,
     out,
     WV, WG, WO, X0, PJ, X1, NB, AV, AG, GF, FT, FR, CV, S1, S2, ACT, STB, SC, PG, T1, T2, R1, R2, OWN,
-    wsend, wrecv, dsend, drecv, asend, arecv, rsend, rrecv, ssend, srecv, gsend, grecv, fsend, frecv,
+    esend, erecv, wsend, wrecv, dsend, drecv, asend, arecv, rsend, rrecv, ssend, srecv, gsend, grecv, fsend, frecv,
 ):
     s = lax.axis_index("sp")
     x = lax.axis_index("tp")
@@ -94,8 +94,7 @@
     if g.nc > 1:
         greet.append((partner, None))
     for axis in ("y", "z"):
-        if size[axis] > 1:
-            greet += [(ring_sp(axis, 1), None), (ring_sp(axis, -1), None)]
+        greet += [(ring_sp(axis, k), None) for k in range(1, size[axis])]
     for sp, tp in greet:
         pl.semaphore_signal(
             barrier, inc=1,
@@ -106,83 +105,104 @@
 
     order = (("y", "z"), ("z", "y"))
     lanes = g.ch // 2
+    pieces = {0: (0, 1), 1: (2,), 2: (3, 4), 3: (5,)}
 
     def source(item, stream):
         if item % 2 == 0:
             return (WV, WG)[stream], pl.ds(0, g.ch)
         return WO, pl.ds(stream * lanes, lanes)
 
-    def block(item, stream, phase, pos, core):
+    def own_slot(item, stream, pos):
         buf, cols = source(item, stream)
-        layer = item // 2
-        if phase == 0:
-            zz, yy = (z, pos) if stream == 0 else (pos, y)
-            return buf.at[zz, yy, core, layer, :, cols]
+        zz, yy = (z, pos) if stream == 0 else (pos, y)
+        return buf.at[zz, yy, c, item // 2, :, cols]
+
+    def block(item, stream, pos, core, piece=None):
+        buf, cols = source(item, stream)
+        across_dim = slice(None)
+        if piece is not None and len(pieces[item]) == 2:
+            n = size[order[stream][0]] // 2
+            near = lax.div(here[order[stream][0]], n)
+            across_dim = pl.ds((near if piece == pieces[item][0] else 1 - near) * n, n)
         if stream == 0:
-            return buf.at[pos, :, core, layer, :, cols]
-        return buf.at[:, pos, core, layer, :, cols]
+            return buf.at[pos, across_dim, core, item // 2, :, cols]
+        return buf.at[across_dim, pos, core, item // 2, :, cols]
 
     def hops(axis):
         n = size[axis]
         return (n // 2, n - 1 - n // 2)
 
-    def ring_copy(item, stream, phase, way, step):
-        axis = order[stream][phase]
+    def scatter_copy(item, stream, k):
+        axis = order[stream][0]
+        ref = own_slot(item, stream, here[axis])
+        return remote(ref, ref, esend.at[item, stream, k], erecv.at[item, stream, k], sp=ring_sp(axis, k))
+
+    def farthest_first(n):
+        return sorted(range(1, n), key=lambda k: -min(k, n - k))
+
+    def scatter(item):
+        for k in farthest_first(max(g.ny, g.nz)):
+            for stream in range(2):
+                if k < size[order[stream][0]]:
+                    go(scatter_copy(item, stream, k))
+
+    def scattered(item):
+        for stream in range(2):
+            axis = order[stream][0]
+            for k in range(1, size[axis]):
+                ref = own_slot(item, stream, moved(axis, -k))
+                remote(
+                    ref, ref, esend.at[item, stream, k], erecv.at[item, stream, k], sp=ring_sp(axis, k)
+                ).wait_recv()
+
+    def ring_copy(item, piece, stream, way, step, back):
+        axis = order[stream][1]
         toward = sgn if way == 0 else -sgn
-        ref = block(item, stream, phase, moved(axis, -toward * step), c)
+        ref = block(item, stream, moved(axis, -toward * (step + back)), c, piece)
         return remote(
             ref, ref,
-            wsend.at[item, stream, phase, way, step],
-            wrecv.at[item, stream, phase, way, step],
+            wsend.at[piece, stream, way, step],
+            wrecv.at[piece, stream, way, step],
             sp=ring_sp(axis, toward),
         )
 
-    def arrival(item, stream, phase, way, step):
-        axis = order[stream][phase]
-        toward = sgn if way == 0 else -sgn
-        ref = block(item, stream, phase, moved(axis, -toward * (step + 1)), c)
-        remote(
-            ref, ref,
-            wsend.at[item, stream, phase, way, step],
-            wrecv.at[item, stream, phase, way, step],
-            sp=ring_sp(axis, toward),
-        ).wait_recv()
-
     def across(item, stream, index, pos):
         if g.nc > 1:
-            ref = block(item, stream, 1, pos, c)
+            ref = block(item, stream, pos, c)
             go(remote(ref, ref, dsend.at[item, stream, index], drecv.at[item, stream, index], sp=partner))
 
-    def begin(item, phase):
+    def begin(item):
+        for piece in pieces[item]:
+            for stream in range(2):
+                axis = order[stream][1]
+                for way in range(2):
+                    if hops(axis)[way] > 0:
+                        go(ring_copy(item, piece, stream, way, 0, 0))
         for stream in range(2):
-            axis = order[stream][phase]
-            for way in range(2):
-                if hops(axis)[way] > 0:
-                    go(ring_copy(item, stream, phase, way, 0))
-            if phase == 1:
-                across(item, stream, 0, here[axis])
-
-    def advance(item, phase, step):
-        for stream in range(2):
-            axis = order[stream][phase]
-            for way in range(2):
-                if step < hops(axis)[way]:
-                    arrival(item, stream, phase, way, step)
-                    if step + 1 < hops(axis)[way]:
-                        go(ring_copy(item, stream, phase, way, step + 1))
-                    if phase == 1:
-                        toward = sgn if way == 0 else -sgn
-                        across(
-                            item, stream, 1 + way * hops(axis)[0] + step,
-                            moved(axis, -toward * (step + 1)),
-                        )
+            across(item, stream, 0, here[order[stream][1]])
+
+    def advance(item, step):
+        for piece in pieces[item]:
+            for stream in range(2):
+                axis = order[stream][1]
+                for way in range(2):
+                    if step < hops(axis)[way]:
+                        ring_copy(item, piece, stream, way, step, 1).wait_recv()
+                        if step + 1 < hops(axis)[way]:
+                            go(ring_copy(item, piece, stream, way, step + 1, 0))
+                        if piece == pieces[item][-1]:
+                            toward = sgn if way == 0 else -sgn
+                            across(
+                                item, stream, 1 + way * hops(axis)[0] + step,
+                                moved(axis, -toward * (step + 1)),
+                            )
 
     def finish(item):
         if g.nc > 1:
             for stream in range(2):
                 axis = order[stream][1]
                 for index in range(size[axis]):
-                    ref = block(item, stream, 1, index, 1 - c)
+                    ref = block(item, stream, index, 1 - c)
                     remote(
                         ref, ref, dsend.at[item, stream, index], drecv.at[item, stream, index], sp=partner
                     ).wait_recv()
@@ -238,24 +258,20 @@
     def as_columns(which, row):
         SC[which] = jnp.transpose(jnp.broadcast_to(row, (128, g.rp)))
 
-    for item in (0, 1):
-        begin(item, 0)
+    scatter(0)
     spread_begin(0, X0)
-    for item in (2, 3):
-        begin(item, 0)
+    scatter(1)
     for j in range(1, g.nx):
         go(remote(PG.at[x], PG.at[x], gsend.at[j - 1], grecv.at[j - 1], tp=at_x(j)))
-    for step in range(steps):
-        for item in (0, 1):
-            advance(item, 0, step)
-    begin(0, 1)
-    begin(1, 1)
+    scattered(0)
+    begin(0)
+    scattered(1)
+    begin(1)
+    scatter(2)
+    scatter(3)
     spread_relay(0, X0)
-    for step in range(steps):
-        for item in (2, 3):
-            advance(item, 0, step)
-    advance(0, 1, 0)
-    advance(1, 1, 0)
+    advance(0, 0)
+    advance(1, 0)
     spread_end(0, X0)
 
     def norm_rows(layer):
@@ -315,7 +331,7 @@
             acc = jnp.zeros((g.rb, 128), F32)
             for tap in range(g.taps):
                 rows = pl.ds(i * g.rb + (HALO - g.taps + 1 + tap), g.rb)
-                acc = acc + taps[layer, tap : tap + 1, cols] * GF[k, rows, :]
+                acc = acc + taps[tap, layer : layer + 1, cols] * GF[k, rows, :]
             CV[k, pl.ds(i * g.rb, g.rb), :] = acc
             whole = [whole[0] + acc, whole[1] + acc * acc]
         S1[pl.ds(i * g.rb, g.rb), :] = whole[0]
@@ -343,13 +359,9 @@
 
         lax.fori_loop(lo, hi, at, 0)
 
-    pending = []
-    for step in range(1, steps):
-        pending.append([lambda st=step, it=it: advance(it, 1, st) for it in (0, 1)])
-    pump_first = pending
-    later = [lambda: (begin(2, 1), begin(3, 1))]
+    later = [lambda: (scattered(2), begin(2), scattered(3), begin(3))]
     for step in range(steps):
-        later += [lambda st=step: advance(2, 1, st), lambda st=step: advance(3, 1, st)]
+        later += [lambda st=step: advance(2, st), lambda st=step: advance(3, st)]
 
     def pump(n):
         for _ in range(n):
@@ -362,9 +374,9 @@
             spread_end(1, PJ)
         norm_rows(layer)
         if layer == 0:
-            for group in pump_first:
-                for event in group:
-                    event()
+            for step in range(1, steps):
+                advance(0, step)
+                advance(1, step)
             pump(1)
             finish(0)
             finish(1)
@@ -472,6 +484,7 @@
 
 def local(g, tokens, pre_gain, w_value, w_gate, taps, norm_gain, norm_shift, w_out, post_gain):
     w_out = jnp.swapaxes(w_out, 1, 2)
+    taps = jnp.swapaxes(taps, 0, 1)
     vm = pl.BlockSpec(memory_space=pltpu.VMEM)
     slots = (g.nz, g.ny, g.nc, 2, g.kr, g.ch)
     rows, ch = g.rows, g.ch
@@ -502,8 +515,10 @@
         pltpu.VMEM((2, 2, rows // 2, ch), BF16),
         pltpu.VMEM((2, 2, rows, ch), BF16),
         pltpu.VMEM((rows, ch), F32),
-        dma((4, 2, 2, 2, most // 2)),
-        dma((4, 2, 2, 2, most // 2)),
+        dma((4, 2, most)),
+        dma((4, 2, most)),
+        dma((6, 2, 2, most // 2)),
+        dma((6, 2, 2, most // 2)),
         dma((4, 2, most)),
         dma((4, 2, most)),
         dma((2, 2, 3)),

time: 140 us -> 127 us (0.907)
  the two profiles are of different devices: /device:TPU:2 before, /device:TPU:8 now
where the time goes in v2:
time: 127 us
  Pallas kernels  125 us (98%)
  local copies, waits for them, and re-layouts  1.72 us (1%)
    pallas_call x1, Pallas kernels, local(): pl.pallas_call(functools.partial(body, g), out_shape=jax.ShapeDtypeStruct...  125 us

profile of v2, /device:TPU:8, one launch (start us, length us, event | category | flops | bytes accessed | tf_op | source)
XLA Modules:
  0.0 127.1 jit_solution(12313430003917634803)
XLA Ops:
  0.0 125.4 %shard_map.91 = bf16[320,512]{1,0:T(8,128)(2,1)} custom-call(bf16[320,512]{1,0:T(8,128)(2,1)} %tok.1, f32[2,2048]{1,0:T(2,128)} %pre_gain.1, bf16[2,16,512]{2,1,0:T(8,128)(2,1)} %wv.1, bf16[2,16,512]{2,1,0:T(8,128)(2,1)} %wg.1, f32[31,2,512]{2,1,0:T(2,128)} %bitcast.2, f32[2,512]{1,0:T(2,128)} %ngain.1, f32[2,512]{1,0:T(2,128)} %nshift.1, ...), custom_call_target="tpu_custom_call" | custom-call | tf_op jit(solution)/shard_map/pallas_call | solution.py:535
  125.4 1.7 %copy.11 = bf16[320,512]{1,0:T(8,128)(2,1)} copy(bf16[320,512]{1,0:T(8,128)(2,1)} %shard_map.91) | data formatting | bytes 655360

commit v3 on v2

--- a/solution.py
+++ b/solution.py
@@ -23,16 +23,19 @@
         self.nsp = nz * ny * nc
         self.kr = self.d // self.nsp
         self.strips = ch // 128
-        self.rp = -(-rows // 128) * 128
         self.rb = 64
         self.blocks = rows // self.rb
+        first = self.blocks - self.blocks // 2
+        self.split = (self.blocks - first) * self.rb
+        self.chunks = tuple((lo, n, -(-n // 128) * 128) for lo, n in ((self.split, rows - self.split), (0, self.split)))
+        self.wide = max(w for _, _, w in self.chunks)
 
 
 def body(
     g,
     tok, pre_gain, wv, wg, taps, ngain, nshift, wo, pgain,
     out,
-    WV, WG, WO, X0, PJ, X1, NB, AV, AG, GF, FT, FR, CV, S1, S2, ACT, STB, SC, PG, T1, T2, R1, R2, OWN,
+    WV, WG, WO, X0, PJ, X1, NB, AV, AG, GF, FT, FR, CV, S1, S2, ACT, STB, SC, PG, T1, T2, R1, R2, OWN, PQ,
     esend, erecv, wsend, wrecv, dsend, drecv, asend, arecv, rsend, rrecv, ssend, srecv, gsend, grecv, fsend, frecv,
 ):
     s = lax.axis_index("sp")
@@ -41,8 +44,12 @@
     y = lax.rem(lax.div(s, g.nc), g.ny)
     z = lax.div(s, g.nc * g.ny)
     sgn = 1 - 2 * c
-    half = g.rows // 2
-    top, bottom = pl.ds(0, half), pl.ds(half, half)
+
+    def rows_of(q, part=None):
+        lo, n, _ = g.chunks[q]
+        if part is None:
+            return pl.ds(lo, n)
+        return pl.ds(lo + part * (n // 2), n // 2)
 
     def sp_of(zz, yy, cc):
         return (zz * g.ny + yy) * g.nc + cc
@@ -209,38 +216,28 @@
 
     steps = max(g.ny, g.nz) // 2
 
-    ways = ((1, top, bottom), (-1, bottom, top))
-
-    def spread_copy(layer, buf, way, piece):
-        toward, first, second = ways[way]
-        slot, part = ((x, first), (x, second), (at_x(-toward), first))[piece]
-        ref = buf.at[slot, part]
+    def spread_copy(layer, q, buf, way, piece, back):
+        toward = 1 - 2 * way
+        origin = at_x(-toward * (back + (piece == 2)))
+        ref = buf.at[origin, rows_of(q, 1 - way if piece == 1 else way)]
         return remote(
-            ref, ref, asend.at[layer, way, piece], arecv.at[layer, way, piece], tp=at_x(toward)
+            ref, ref, asend.at[layer, q, way, piece], arecv.at[layer, q, way, piece], tp=at_x(toward)
         )
 
-    def spread_begin(layer, buf):
+    def spread_begin(layer, q, buf):
         for piece in range(2):
             for way in range(2):
-                go(spread_copy(layer, buf, way, piece))
-
-    def spread_wait(layer, buf, way, piece):
-        toward, first, second = ways[way]
-        slot, part = ((at_x(-toward), first), (at_x(-toward), second), (at_x(-2 * toward), first))[piece]
-        ref = buf.at[slot, part]
-        remote(
-            ref, ref, asend.at[layer, way, piece], arecv.at[layer, way, piece], tp=at_x(toward)
-        ).wait_recv()
-
-    def spread_relay(layer, buf):
+                go(spread_copy(layer, q, buf, way, piece, 0))
+
+    def spread_relay(layer, q, buf):
         for way in range(2):
-            spread_wait(layer, buf, way, 0)
-            go(spread_copy(layer, buf, way, 2))
-
-    def spread_end(layer, buf):
+            spread_copy(layer, q, buf, way, 0, 1).wait_recv()
+            go(spread_copy(layer, q, buf, way, 2, 0))
+
+    def spread_end(layer, q, buf):
         for piece in (1, 2):
             for way in range(2):
-                spread_wait(layer, buf, way, piece)
+                spread_copy(layer, q, buf, way, piece, 1).wait_recv()
 
     def tell(which):
         for j in range(1, g.nx):
@@ -252,14 +249,17 @@
             ref = STB.at[which, at_x(-j)]
             remote(ref, ref, ssend.at[which, j - 1], srecv.at[which, j - 1], tp=at_x(j)).wait_recv()
 
-    def row_sums(buf):
-        return jnp.sum(jnp.transpose(buf[...]), axis=0, keepdims=True)
-
-    def as_columns(which, row):
-        SC[which] = jnp.transpose(jnp.broadcast_to(row, (128, g.rp)))
+    def put_sums(which, row, buf, q):
+        w = g.chunks[q][2]
+        STB[which, x, row : row + 1, 0:w] = jnp.sum(jnp.transpose(buf[q, 0:w, :]), axis=0, keepdims=True)
+
+    def as_columns(q, k, row):
+        w = g.chunks[q][2]
+        SC[q, k, 0:w, :] = jnp.transpose(jnp.broadcast_to(row, (128, w)))
 
     scatter(0)
-    spread_begin(0, X0)
+    for q in range(2):
+        spread_begin(0, q, X0)
     scatter(1)
     for j in range(1, g.nx):
         go(remote(PG.at[x], PG.at[x], gsend.at[j - 1], grecv.at[j - 1], tp=at_x(j)))
@@ -269,62 +269,83 @@
     begin(1)
     scatter(2)
     scatter(3)
-    spread_relay(0, X0)
+    for q in range(2):
+        spread_relay(0, q, X0)
     advance(0, 0)
     advance(1, 0)
-    spread_end(0, X0)
-
-    def norm_rows(layer):
+    for q in range(2):
+        spread_end(0, q, X0)
+
+    def loop(fn, lo, hi):
         def at(i, carry):
-            rows = pl.ds(i * g.rb, g.rb)
+            fn(i)
+            return carry
+
+        lax.fori_loop(lo, hi, at, 0)
+
+    def over(q, fn):
+        lo, n, _ = g.chunks[q]
+        loop(fn, lo // g.rb, (lo + n) // g.rb)
+
+    def norm_rows(layer, i):
+        rows = pl.ds(i * g.rb, g.rb)
+        if layer == 1:
+            square = jnp.zeros((g.rb, 1), F32)
+            for j in range(g.nx):
+                v = PJ[j, rows, :].astype(F32)
+                square += jnp.sum(v * v, -1, keepdims=True)
+            scale = lax.rsqrt(square / g.d + EPSILON)
+        total = jnp.zeros((g.rb, 1), F32)
+        for j in range(g.nx):
+            v = X0[j, rows, :].astype(F32)
             if layer == 1:
-                square = jnp.zeros((g.rb, 1), F32)
-                for j in range(g.nx):
-                    v = PJ[j, rows, :].astype(F32)
-                    square += jnp.sum(v * v, -1, keepdims=True)
-                scale = lax.rsqrt(square / g.d + EPSILON)
-            total = jnp.zeros((g.rb, 1), F32)
-            for j in range(g.nx):
-                v = X0[j, rows, :].astype(F32)
-                if layer == 1:
-                    v = v + PJ[j, rows, :].astype(F32) * scale * PG[j, 0:1, :]
-                    X1[j, rows, :] = v.astype(BF16)
-                    v = v.astype(BF16).astype(F32)
-                total += jnp.sum(v * v, -1, keepdims=True)
-            inv = lax.rsqrt(total / g.d + EPSILON)
-            for j in range(g.nx):
-                v = (X0, X1)[layer][j, rows, :].astype(F32)
-                cols = pl.ds(j * g.ch, g.ch)
-                NB[j, rows, :] = (v * inv * pre_gain[layer : layer + 1, cols]).astype(BF16)
-            return carry
-
-        lax.fori_loop(0, g.blocks, at, 0)
+                v = v + PJ[j, rows, :].astype(F32) * scale * PG[j, 0:1, :]
+                X1[j, rows, :] = v.astype(BF16)
+                v = v.astype(BF16).astype(F32)
+            total += jnp.sum(v * v, -1, keepdims=True)
+        inv = lax.rsqrt(total / g.d + EPSILON)
+        for j in range(g.nx):
+            v = (X0, X1)[layer][j, rows, :].astype(F32)
+            cols = pl.ds(j * g.ch, g.ch)
+            NB[j, rows, :] = (v * inv * pre_gain[layer : layer + 1, cols]).astype(BF16)
 
     zs = g.nz // g.nx
 
-    def project_in(layer):
-        for n, (acc, w) in enumerate(((AV, WV), (AG, WG))):
+    def project_in(layer, rows):
+        for acc, w in ((AV, WV), (AG, WG)):
+            def term(j):
+                mat = w[pl.ds(j * zs, zs), :, :, layer].reshape(g.ch, g.ch)
+                return jnp.dot(NB[j, rows, :], mat, preferred_element_type=F32)
+
             def at(j, carry):
-                mat = w[pl.ds(j * zs, zs), :, :, layer].reshape(g.ch, g.ch)
-                acc[...] += jnp.dot(NB[j], mat, preferred_element_type=F32)
+                acc[rows, :] += term(j)
                 return carry
 
-            mat = w[0:zs, :, :, layer].reshape(g.ch, g.ch)
-            acc[...] = jnp.dot(NB[0], mat, preferred_element_type=F32)
+            acc[rows, :] = term(0)
             lax.fori_loop(1, g.nx, at, 0)
 
-    def gate(i, carry):
+    def gate(i):
         rows = pl.ds(i * g.rb, g.rb)
         for k in range(g.strips):
             cols = pl.ds(k * 128, 128)
             act = (AV[rows, cols] * jax.nn.sigmoid(AG[rows, cols])).astype(BF16)
             GF[k, pl.ds(HALO + i * g.rb, g.rb), :] = act.astype(F32)
-        return carry
 
     def fringe_copy(layer):
         return remote(FT.at[layer], FR.at[layer], fsend.at[layer], frecv.at[layer], sp=after)
 
-    def convolve(layer, i):
+    def fringe_send(layer):
+        for k in range(g.strips):
+            FT[layer, :, k * 128 : (k + 1) * 128] = GF[k, g.rows : g.rows + HALO, :].astype(BF16)
+        go(fringe_copy(layer))
+
+    def fringe_take(layer):
+        fringe_copy(layer).wait_recv()
+        keep = jnp.where(s > 0, 1.0, 0.0).astype(F32)
+        for k in range(g.strips):
+            GF[k, 0:HALO, :] = FR[layer, :, k * 128 : (k + 1) * 128].astype(F32) * keep
+
+    def convolve(layer, q, i):
         whole = [jnp.zeros((g.rb, 128), F32) for _ in range(2)]
         for k in range(g.strips):
             cols = pl.ds(k * 128, 128)
@@ -334,13 +355,15 @@
                 acc = acc + taps[tap, layer : layer + 1, cols] * GF[k, rows, :]
             CV[k, pl.ds(i * g.rb, g.rb), :] = acc
             whole = [whole[0] + acc, whole[1] + acc * acc]
-        S1[pl.ds(i * g.rb, g.rb), :] = whole[0]
-        S2[pl.ds(i * g.rb, g.rb), :] = whole[1]
-
-    def activate(layer, i):
+        local_rows = pl.ds(i * g.rb - g.chunks[q][0], g.rb)
+        S1[q, local_rows, :] = whole[0]
+        S2[q, local_rows, :] = whole[1]
+
+    def activate(layer, q, i):
         rows = pl.ds(i * g.rb, g.rb)
-        center = SC[0, rows, :]
-        inv = SC[1, rows, :]
+        local_rows = pl.ds(i * g.rb - g.chunks[q][0], g.rb)
+        center = SC[q, 0, local_rows, :]
+        inv = SC[q, 1, local_rows, :]
         for k in range(g.strips):
             cols = pl.ds(k * 128, 128)
             v = (CV[k, rows, :] - center) * inv * ngain[layer : layer + 1, cols] + nshift[
@@ -348,136 +371,164 @@
             ]
             ACT[rows, cols] = (v * jax.nn.sigmoid(v)).astype(BF16)
 
-    def part_for(layer, dest):
+    def stats_send(layer, q):
+        put_sums(2 * layer + q, 0, S1, q)
+        put_sums(2 * layer + q, 1, S2, q)
+        tell(2 * layer + q)
+
+    def stats_take(layer, q):
+        which, w = 2 * layer + q, g.chunks[q][2]
+        told(which)
+        sums = STB[which, 0, :, 0:w]
+        for j in range(1, g.nx):
+            sums = sums + STB[which, j, :, 0:w]
+        center = sums[0:1, :] / g.d
+        spread = jnp.maximum(sums[1:2, :] / g.d - center * center, 0.0)
+        as_columns(q, 0, center)
+        as_columns(q, 1, lax.rsqrt(spread + LN_EPSILON))
+
+    def part_for(layer, q, dest):
         mat = WO[pl.ds(dest * zs, zs), :, :, layer].reshape(g.ch, g.ch)
-        return lax.dot_general(ACT[...], mat, (((1,), (1,)), ((), ())), preferred_element_type=F32)
-
-    def loop(fn, lo, hi):
-        def at(i, carry):
-            fn(i)
-            return carry
-
-        lax.fori_loop(lo, hi, at, 0)
-
-    later = [lambda: (scattered(2), begin(2), scattered(3), begin(3))]
-    for step in range(steps):
-        later += [lambda st=step: advance(2, st), lambda st=step: advance(3, st)]
-
-    def pump(n):
-        for _ in range(n):
-            if later:
-                later.pop(0)()
-
+        return lax.dot_general(
+            ACT[rows_of(q), :], mat, (((1,), (1,)), ((), ())), preferred_element_type=F32
+        )
+
+    def far_hop(layer, q, way):
+        part = rows_of(q, way)
+        return remote(
+            T1.at[layer, part], R1.at[layer, way, part],
+            rsend.at[layer, q, way], rrecv.at[layer, q, way], tp=at_x(1 - 2 * way),
+        )
+
+    def near_hop(layer, q, way, added):
+        part = rows_of(q, way if added else 1 - way)
+        index = 2 + 2 * way + added
+        return remote(
+            T2.at[layer, way, part], R2.at[layer, way, part],
+            rsend.at[layer, q, index], rrecv.at[layer, q, index], tp=at_x(1 - 2 * way),
+        )
+
+    def shares(layer, q):
+        T1[layer, rows_of(q)] = part_for(layer, q, at_x(2)).astype(BF16)
+        for way in range(2):
+            go(far_hop(layer, q, way))
+        for way in range(2):
+            OWN[way, rows_of(q)] = part_for(layer, q, at_x(1 - 2 * way))
+            part = rows_of(q, 1 - way)
+            T2[layer, way, part] = OWN[way, part].astype(BF16)
+            go(near_hop(layer, q, way, 0))
+
+    def relay_shares(layer, q):
+        for way in range(2):
+            far_hop(layer, q, way).wait_recv()
+            part = rows_of(q, way)
+            T2[layer, way, part] = (OWN[way, part] + R1[layer, way, part].astype(F32)).astype(BF16)
+            go(near_hop(layer, q, way, 1))
+
+    def own_share(layer, q):
+        OWN[2, rows_of(q)] = part_for(layer, q, x)
+
+    def shares_end(layer, q):
+        for added in range(2):
+            for way in range(2):
+                near_hop(layer, q, way, added).wait_recv()
+
+        def combine(i):
+            rows = pl.ds(i * g.rb, g.rb)
+            v = (OWN[2, rows] + R2[layer, 0, rows].astype(F32) + R2[layer, 1, rows].astype(F32)).astype(BF16)
+            if layer == 0:
+                PJ[x, rows, :] = v
+            else:
+                PQ[rows, :] = v
+                v = v.astype(F32)
+                v = v * v
+                S1[q, pl.ds(i * g.rb - g.chunks[q][0], g.rb), :] = sum(
+                    v[:, k * 128 : (k + 1) * 128] for k in range(g.strips)
+                )
+
+        over(q, combine)
+
+    A, B = 0, 1
     for layer in range(2):
-        if layer == 1:
-            spread_relay(1, PJ)
-            spread_end(1, PJ)
-        norm_rows(layer)
         if layer == 0:
+            loop(lambda i: norm_rows(0, i), 0, g.blocks)
             for step in range(1, steps):
                 advance(0, step)
                 advance(1, step)
-            pump(1)
+            scattered(2)
+            begin(2)
+            scattered(3)
+            begin(3)
             finish(0)
+            project_in(0, pl.ds(0, g.rows))
             finish(1)
+            over(A, gate)
+            fringe_send(0)
+            over(B, gate)
         else:
-            pump(len(later))
+            spread_end(1, A, PJ)
+            over(A, lambda i: norm_rows(1, i))
             finish(2)
+            project_in(1, rows_of(A))
+            over(A, gate)
+            fringe_send(1)
+            spread_end(1, B, PJ)
+            over(B, lambda i: norm_rows(1, i))
+            project_in(1, rows_of(B))
+            over(B, gate)
             finish(3)
-        project_in(layer)
-        lax.fori_loop(0, g.blocks, gate, 0)
-        for k in range(g.strips):
-            FT[layer, :, k * 128 : (k + 1) * 128] = GF[k, g.rows : g.rows + HALO, :].astype(BF16)
+        over(A, lambda i: convolve(layer, A, i))
+        stats_send(layer, A)
+        loop(lambda i: convolve(layer, B, i), 1, g.split // g.rb)
+        fringe_take(layer)
+        loop(lambda i: convolve(layer, B, i), 0, 1)
+        stats_send(layer, B)
         if layer == 0:
-            pump(2)
-        go(fringe_copy(layer))
-        loop(lambda i: convolve(layer, i), 1, g.blocks)
-        fringe_copy(layer).wait_recv()
-        keep = jnp.where(s > 0, 1.0, 0.0).astype(F32)
-        for k in range(g.strips):
-            GF[k, 0:HALO, :] = FR[layer, :, k * 128 : (k + 1) * 128].astype(F32) * keep
-        loop(lambda i: convolve(layer, i), 0, 1)
-        STB[layer, x, 0:1, :] = row_sums(S1)
-        STB[layer, x, 1:2, :] = row_sums(S2)
-        tell(layer)
+            advance(2, 0)
+            advance(3, 0)
+        stats_take(layer, A)
+        over(A, lambda i: activate(layer, A, i))
+        shares(layer, A)
+        stats_take(layer, B)
+        over(B, lambda i: activate(layer, B, i))
+        shares(layer, B)
+        relay_shares(layer, A)
         if layer == 0:
-            pump(2)
-        told(layer)
-        sums = STB[layer, 0]
-        for j in range(1, g.nx):
-            sums = sums + STB[layer, j]
-        center = sums[0:1, :] / g.d
-        spread = jnp.maximum(sums[1:2, :] / g.d - center * center, 0.0)
-        as_columns(0, center)
-        as_columns(1, lax.rsqrt(spread + LN_EPSILON))
-        loop(lambda i: activate(layer, i), 0, g.blocks)
-
-        def rs(index, src, dst, toward):
-            return remote(src, dst, rsend.at[layer, index], rrecv.at[layer, index], tp=at_x(toward))
-
-        hop = (
-            rs(0, T1.at[layer, top], R1.at[layer, 0], 1),
-            rs(1, T1.at[layer, bottom], R1.at[layer, 1], -1),
-            rs(2, T2.at[layer, 0], R2.at[layer, 0], 1),
-            rs(3, T2.at[layer, 1], R2.at[layer, 1], -1),
-        )
-        T1[layer] = part_for(layer, at_x(2)).astype(BF16)
-        go(hop[0])
-        go(hop[1])
-        OWN[...] = part_for(layer, at_x(1))
-        hop[0].wait_recv()
-        T2[layer, 0, top] = (OWN[top] + R1[layer, 0].astype(F32)).astype(BF16)
-        T2[layer, 0, bottom] = OWN[bottom].astype(BF16)
-        go(hop[2])
-        OWN[...] = part_for(layer, at_x(-1))
-        hop[1].wait_recv()
-        T2[layer, 1, bottom] = (OWN[bottom] + R1[layer, 1].astype(F32)).astype(BF16)
-        T2[layer, 1, top] = OWN[top].astype(BF16)
-        go(hop[3])
-        OWN[...] = part_for(layer, x)
+            advance(2, 1)
+            advance(3, 1)
+        own_share(layer, A)
+        relay_shares(layer, B)
+        own_share(layer, B)
+        for q in (A, B):
+            shares_end(layer, q)
+            if layer == 0:
+                spread_begin(1, q, PJ)
+                advance(2, 2 + q)
+                advance(3, 2 + q)
+            else:
+                put_sums(4 + q, 0, S1, q)
+                tell(4 + q)
         if layer == 0:
-            pump(2)
-        hop[2].wait_recv()
-        hop[3].wait_recv()
-
-        def combine(i):
-            rows = pl.ds(i * g.rb, g.rb)
-            v = (OWN[rows] + R2[layer, 0, rows].astype(F32) + R2[layer, 1, rows].astype(F32)).astype(BF16)
-            if layer == 0:
-                PJ[x, rows, :] = v
-            else:
-                T1[0, rows, :] = v
-                v = v.astype(F32)
-                v = v * v
-                S1[rows, :] = sum(v[:, k * 128 : (k + 1) * 128] for k in range(g.strips))
-
-        if layer == 0:
-            loop(combine, 0, g.blocks)
             for j in range(1, g.nx):
                 ref = PG.at[at_x(-j)]
                 remote(ref, ref, gsend.at[j - 1], grecv.at[j - 1], tp=at_x(j)).wait_recv()
-            spread_begin(1, PJ)
-        else:
-            rs_done = [hop_ for hop_ in sent]
-            for copy in rs_done:
-                copy.wait_send()
-            sent.clear()
-            loop(combine, 0, g.blocks)
-
-    STB[2, x, 0:1, :] = row_sums(S1)
-    tell(2)
-    told(2)
-    square = sum(STB[2, j, 0:1, :] for j in range(g.nx))
-    as_columns(0, lax.rsqrt(square / g.d + EPSILON))
-
-    def last(i):
-        rows = pl.ds(i * g.rb, g.rb)
-        for k in range(g.strips):
-            cols = pl.ds(k * 128, 128)
-            v = T1[0, rows, cols].astype(F32) * SC[0, rows, :] * pgain[1:2, cols]
-            out[rows, cols] = (X1[x, rows, cols].astype(F32) + v).astype(BF16)
-
-    loop(last, 0, g.blocks)
+            for q in (A, B):
+                spread_relay(1, q, PJ)
+
+    for q in (A, B):
+        told(4 + q)
+        square = sum(STB[4 + q, j, 0:1, 0 : g.chunks[q][2]] for j in range(g.nx))
+        as_columns(q, 0, lax.rsqrt(square / g.d + EPSILON))
+
+        def last(i):
+            rows = pl.ds(i * g.rb, g.rb)
+            scale = SC[q, 0, pl.ds(i * g.rb - g.chunks[q][0], g.rb), :]
+            for k in range(g.strips):
+                cols = pl.ds(k * 128, 128)
+                v = PQ[rows, cols].astype(F32) * scale * pgain[1:2, cols]
+                out[rows, cols] = (X1[x, rows, cols].astype(F32) + v).astype(BF16)
+
+        over(q, last)
     for copy in sent:
         copy.wait_send()
 
@@ -504,29 +555,30 @@
         pltpu.VMEM((2, HALO, ch), BF16),
         pltpu.VMEM((2, HALO, ch), BF16),
         pltpu.VMEM((g.strips, rows, 128), F32),
-        pltpu.VMEM((g.rp, 128), F32),
-        pltpu.VMEM((g.rp, 128), F32),
+        pltpu.VMEM((2, g.wide, 128), F32),
+        pltpu.VMEM((2, g.wide, 128), F32),
         pltpu.VMEM((rows, ch), BF16),
-        pltpu.VMEM((3, g.nx, 8, g.rp), F32),
-        pltpu.VMEM((2, g.rp, 128), F32),
+        pltpu.VMEM((6, g.nx, 8, g.wide), F32),
+        pltpu.VMEM((2, 2, g.wide, 128), F32),
         pltpu.VMEM((g.nx, 8, ch), F32),
         pltpu.VMEM((2, rows, ch), BF16),
         pltpu.VMEM((2, 2, rows, ch), BF16),
-        pltpu.VMEM((2, 2, rows // 2, ch), BF16),
         pltpu.VMEM((2, 2, rows, ch), BF16),
-        pltpu.VMEM((rows, ch), F32),
+        pltpu.VMEM((2, 2, rows, ch), BF16),
+        pltpu.VMEM((3, rows, ch), F32),
+        pltpu.VMEM((rows, ch), BF16),
         dma((4, 2, most)),
         dma((4, 2, most)),
         dma((6, 2, 2, most // 2)),
         dma((6, 2, 2, most // 2)),
         dma((4, 2, most)),
         dma((4, 2, most)),
-        dma((2, 2, 3)),
-        dma((2, 2, 3)),
-        dma((2, 4)),
-        dma((2, 4)),
-        dma((3, 3)),
-        dma((3, 3)),
+        dma((2, 2, 2, 3)),
+        dma((2, 2, 2, 3)),
+        dma((2, 2, 6)),
+        dma((2, 2, 6)),
+        dma((6, 3)),
+        dma((6, 3)),
         dma((3,)),
         dma((3,)),
         dma((2,)),

time: 127 us -> 109 us (0.86)
  the two profiles are of different devices: /device:TPU:8 before, /device:TPU:2 now
where the time goes in v3:
time: 109 us
  Pallas kernels  107 us (98%)
  local copies, waits for them, and re-layouts  1.72 us (2%)
    pallas_call x1, Pallas kernels, local(): pl.pallas_call(functools.partial(body, g), out_shape=jax.ShapeDtypeStruct...  107 us

profile of v3, /device:TPU:2, one launch (start us, length us, event | category | flops | bytes accessed | tf_op | source)
XLA Modules:
  0.0 108.7 jit_solution(749424998518497481)
XLA Ops:
  0.0 107.0 %shard_map.91 = bf16[320,512]{1,0:T(8,128)(2,1)} custom-call(bf16[320,512]{1,0:T(8,128)(2,1)} %tok.1, f32[2,2048]{1,0:T(2,128)} %pre_gain.1, bf16[2,16,512]{2,1,0:T(8,128)(2,1)} %wv.1, bf16[2,16,512]{2,1,0:T(8,128)(2,1)} %wg.1, f32[31,2,512]{2,1,0:T(2,128)} %bitcast.2, f32[2,512]{1,0:T(2,128)} %ngain.1, f32[2,512]{1,0:T(2,128)} %nshift.1, ...), custom_call_target="tpu_custom_call" | custom-call | tf_op jit(solution)/shard_map/pallas_call | solution.py:587
  107.0 1.7 %copy.11 = bf16[320,512]{1,0:T(8,128)(2,1)} copy(bf16[320,512]{1,0:T(8,128)(2,1)} %shard_map.91) | data formatting | bytes 655360

commit v4 on v3

--- a/solution.py
+++ b/solution.py
@@ -25,7 +25,7 @@
         self.strips = ch // 128
         self.rb = 64
         self.blocks = rows // self.rb
-        first = self.blocks - self.blocks // 2
+        first = self.blocks // 2
         self.split = (self.blocks - first) * self.rb
         self.chunks = tuple((lo, n, -(-n // 128) * 128) for lo, n in ((self.split, rows - self.split), (0, self.split)))
         self.wide = max(w for _, _, w in self.chunks)
@@ -112,7 +112,7 @@
 
     order = (("y", "z"), ("z", "y"))
     lanes = g.ch // 2
-    pieces = {0: (0, 1), 1: (2,), 2: (3, 4), 3: (5,)}
+    pieces = {0: (0, 1), 1: (2,), 2: (3,), 3: (4,)}
 
     def source(item, stream):
         if item % 2 == 0:
@@ -141,8 +141,14 @@
 
     def scatter_copy(item, stream, k):
         axis = order[stream][0]
-        ref = own_slot(item, stream, here[axis])
-        return remote(ref, ref, esend.at[item, stream, k], erecv.at[item, stream, k], sp=ring_sp(axis, k))
+        if k == 0:
+            buf, cols = source(item, stream)
+            some = pl.ds(0, size[axis] - 1)
+            zz, yy = (z, some) if stream == 0 else (some, y)
+            ref = buf.at[zz, yy, c, item // 2, :, cols]
+        else:
+            ref = own_slot(item, stream, here[axis])
+        return remote(ref, ref, esend.at[item, stream], erecv.at[item, stream], sp=ring_sp(axis, max(k, 1)))
 
     def farthest_first(n):
         return sorted(range(1, n), key=lambda k: -min(k, n - k))
@@ -151,16 +157,15 @@
         for k in farthest_first(max(g.ny, g.nz)):
             for stream in range(2):
                 if k < size[order[stream][0]]:
-                    go(scatter_copy(item, stream, k))
+                    scatter_copy(item, stream, k).start()
+        for stream in range(2):
+            if size[order[stream][0]] > 1:
+                sent.append(scatter_copy(item, stream, 0))
 
     def scattered(item):
         for stream in range(2):
-            axis = order[stream][0]
-            for k in range(1, size[axis]):
-                ref = own_slot(item, stream, moved(axis, -k))
-                remote(
-                    ref, ref, esend.at[item, stream, k], erecv.at[item, stream, k], sp=ring_sp(axis, k)
-                ).wait_recv()
+            if size[order[stream][0]] > 1:
+                scatter_copy(item, stream, 0).wait_recv()
 
     def ring_copy(item, piece, stream, way, step, back):
         axis = order[stream][1]
@@ -168,15 +173,26 @@
         ref = block(item, stream, moved(axis, -toward * (step + back)), c, piece)
         return remote(
             ref, ref,
-            wsend.at[piece, stream, way, step],
+            wsend.at[piece, stream],
             wrecv.at[piece, stream, way, step],
             sp=ring_sp(axis, toward),
         )
 
-    def across(item, stream, index, pos):
-        if g.nc > 1:
+    def ring_sent(item, piece, stream):
+        buf, cols = source(item, stream)
+        first, second = (size[axis] for axis in order[stream])
+        one, some = pl.ds(0, first // len(pieces[item])), pl.ds(0, second - 1)
+        zz, yy = (some, one) if stream == 0 else (one, some)
+        ref = buf.at[zz, yy, c, item // 2, :, cols]
+        return remote(ref, ref, wsend.at[piece, stream], wrecv.at[piece, stream, 0, 0], sp=partner)
+
+    def across(item, stream, pos=None):
+        if pos is None:
+            buf, cols = source(item, stream)
+            ref = buf.at[:, :, c, item // 2, :, cols]
+        else:
             ref = block(item, stream, pos, c)
-            go(remote(ref, ref, dsend.at[item, stream, index], drecv.at[item, stream, index], sp=partner))
+        return remote(ref, ref, dsend.at[item, stream], drecv.at[item, stream], sp=partner)
 
     def begin(item):
         for piece in pieces[item]:
@@ -184,9 +200,12 @@
                 axis = order[stream][1]
                 for way in range(2):
                     if hops(axis)[way] > 0:
-                        go(ring_copy(item, piece, stream, way, 0, 0))
-        for stream in range(2):
-            across(item, stream, 0, here[order[stream][1]])
+                        ring_copy(item, piece, stream, way, 0, 0).start()
+                if size[axis] > 1:
+                    sent.append(ring_sent(item, piece, stream))
+        if g.nc > 1 and item < 2:
+            for stream in range(2):
+                across(item, stream, here[order[stream][1]]).start()
 
     def advance(item, step):
         for piece in pieces[item]:
@@ -196,23 +215,22 @@
                     if step < hops(axis)[way]:
                         ring_copy(item, piece, stream, way, step, 1).wait_recv()
                         if step + 1 < hops(axis)[way]:
-                            go(ring_copy(item, piece, stream, way, step + 1, 0))
-                        if piece == pieces[item][-1]:
+                            ring_copy(item, piece, stream, way, step + 1, 0).start()
+                        if g.nc > 1 and item < 2 and piece == pieces[item][-1]:
                             toward = sgn if way == 0 else -sgn
-                            across(
-                                item, stream, 1 + way * hops(axis)[0] + step,
-                                moved(axis, -toward * (step + 1)),
-                            )
+                            across(item, stream, moved(axis, -toward * (step + 1))).start()
+        if step == steps - 1 and g.nc > 1:
+            for stream in range(2):
+                if item >= 2:
+                    across(item, stream).start()
+                sent.append(across(item, stream))
 
     def finish(item):
         if g.nc > 1:
             for stream in range(2):
-                axis = order[stream][1]
-                for index in range(size[axis]):
-                    ref = block(item, stream, index, 1 - c)
-                    remote(
-                        ref, ref, dsend.at[item, stream, index], drecv.at[item, stream, index], sp=partner
-                    ).wait_recv()
+                buf, cols = source(item, stream)
+                ref = buf.at[:, :, 1 - c, item // 2, :, cols]
+                remote(ref, ref, dsend.at[item, stream], drecv.at[item, stream], sp=partner).wait_recv()
 
     steps = max(g.ny, g.nz) // 2
 
@@ -567,12 +585,12 @@
         pltpu.VMEM((2, 2, rows, ch), BF16),
         pltpu.VMEM((3, rows, ch), F32),
         pltpu.VMEM((rows, ch), BF16),
-        dma((4, 2, most)),
-        dma((4, 2, most)),
-        dma((6, 2, 2, most // 2)),
-        dma((6, 2, 2, most // 2)),
-        dma((4, 2, most)),
-        dma((4, 2, most)),
+        dma((4, 2)),
+        dma((4, 2)),
+        dma((5, 2)),
+        dma((5, 2, 2, most // 2)),
+        dma((4, 2)),
+        dma((4, 2)),
         dma((2, 2, 2, 3)),
         dma((2, 2, 2, 3)),
         dma((2, 2, 6)),

time: 109 us -> 106 us (0.972)
  the two profiles are of different devices: /device:TPU:2 before, /device:TPU:8 now
where the time goes in v4:
time: 106 us; the launch traced here: 105 us
  Pallas kernels  104 us (98%)
  local copies, waits for them, and re-layouts  1.72 us (2%)
    pallas_call x1, Pallas kernels, local(): pl.pallas_call(functools.partial(body, g), out_shape=jax.ShapeDtypeStruct...  104 us

profile of v4, /device:TPU:8, one launch (start us, length us, event | category | flops | bytes accessed | tf_op | source)
XLA Modules:
  0.0 105.4 jit_solution(18044936521525063356)
XLA Ops:
  0.0 103.7 %shard_map.91 = bf16[320,512]{1,0:T(8,128)(2,1)} custom-call(bf16[320,512]{1,0:T(8,128)(2,1)} %tok.1, f32[2,2048]{1,0:T(2,128)} %pre_gain.1, bf16[2,16,512]{2,1,0:T(8,128)(2,1)} %wv.1, bf16[2,16,512]{2,1,0:T(8,128)(2,1)} %wg.1, f32[31,2,512]{2,1,0:T(2,128)} %bitcast.2, f32[2,512]{1,0:T(2,128)} %ngain.1, f32[2,512]{1,0:T(2,128)} %nshift.1, ...), custom_call_target="tpu_custom_call" | custom-call | tf_op jit(solution)/shard_map/pallas_call | solution.py:605
  103.7 1.7 %copy.11 = bf16[320,512]{1,0:T(8,128)(2,1)} copy(bf16[320,512]{1,0:T(8,128)(2,1)} %shard_map.91) | data formatting | bytes 655360

commit v5 on v4

--- a/solution.py
+++ b/solution.py
@@ -33,9 +33,9 @@
 
 def body(
     g,
-    tok, pre_gain, wv, wg, taps, ngain, nshift, wo, pgain,
+    tok, pre_gain, wv, wg, hbm_taps, ngain, nshift, wo, pgain,
     out,
-    WV, WG, WO, X0, PJ, X1, NB, AV, AG, GF, FT, FR, CV, S1, S2, ACT, STB, SC, PG, T1, T2, R1, R2, OWN, PQ,
+    WV, WG, WO, X0, PJ, X1, NB, AV, AG, GF, FT, FR, CV, S1, S2, ACT, STB, SC, PG, T1, T2, R1, R2, OWN, PQ, taps, lsem,
     esend, erecv, wsend, wrecv, dsend, drecv, asend, arecv, rsend, rrecv, ssend, srecv, gsend, grecv, fsend, frecv,
 ):
     s = lax.axis_index("sp")
@@ -85,15 +85,14 @@
     after = lax.rem(s + 1, g.nsp)
     before = lax.rem(s + g.nsp - 1, g.nsp)
 
-    for layer in range(2):
-        WV[z, y, c, layer] = wv[layer]
-        WG[z, y, c, layer] = wg[layer]
-        WO[z, y, c, layer] = wo[layer]
-    PG[x] = jnp.broadcast_to(pgain[0:1, :], (8, g.ch))
-    X0[x] = tok[...]
-    STB[...] = jnp.zeros_like(STB)
-    S1[...] = jnp.zeros_like(S1)
-    S2[...] = jnp.zeros_like(S2)
+    loads = [(wv.at[i], WV.at[z, y, c, i]) for i in range(2)]
+    loads += [(wg.at[i], WG.at[z, y, c, i]) for i in range(2)]
+    loads += [(tok, X0.at[x])]
+    loads += [(wo.at[i], WO.at[z, y, c, i]) for i in range(2)]
+    loads += [(hbm_taps, taps)]
+    loads = [pltpu.make_async_copy(a, b, lsem.at[i]) for i, (a, b) in enumerate(loads)]
+    for load in loads:
+        load.start()
 
     barrier = pltpu.get_barrier_semaphore()
     greet = [(None, at_x(j)) for j in range(1, g.nx)]
@@ -108,7 +107,13 @@
             device_id=(s if sp is None else sp, x if tp is None else tp),
             device_id_type=MESH,
         )
+    PG[x] = jnp.broadcast_to(pgain[0:1, :], (8, g.ch))
+    STB[...] = jnp.zeros_like(STB)
+    S1[...] = jnp.zeros_like(S1)
+    S2[...] = jnp.zeros_like(S2)
     pl.semaphore_wait(barrier, len(greet))
+    for load in loads[:-1]:
+        load.wait()
 
     order = (("y", "z"), ("z", "y"))
     lanes = g.ch // 2
@@ -325,22 +330,14 @@
         for j in range(g.nx):
             v = (X0, X1)[layer][j, rows, :].astype(F32)
             cols = pl.ds(j * g.ch, g.ch)
-            NB[j, rows, :] = (v * inv * pre_gain[layer : layer + 1, cols]).astype(BF16)
+            NB[rows, cols] = (v * inv * pre_gain[layer : layer + 1, cols]).astype(BF16)
 
     zs = g.nz // g.nx
 
     def project_in(layer, rows):
         for acc, w in ((AV, WV), (AG, WG)):
-            def term(j):
-                mat = w[pl.ds(j * zs, zs), :, :, layer].reshape(g.ch, g.ch)
-                return jnp.dot(NB[j, rows, :], mat, preferred_element_type=F32)
-
-            def at(j, carry):
-                acc[rows, :] += term(j)
-                return carry
-
-            acc[rows, :] = term(0)
-            lax.fori_loop(1, g.nx, at, 0)
+            mat = w[:, :, :, layer].reshape(g.d, g.ch)
+            acc[rows, :] = jnp.dot(NB[rows, :], mat, preferred_element_type=F32)
 
     def gate(i):
         rows = pl.ds(i * g.rb, g.rb)
@@ -495,6 +492,8 @@
             project_in(1, rows_of(B))
             over(B, gate)
             finish(3)
+        if layer == 0:
+            loads[-1].wait()
         over(A, lambda i: convolve(layer, A, i))
         stats_send(layer, A)
         loop(lambda i: convolve(layer, B, i), 1, g.split // g.rb)
@@ -555,6 +554,7 @@
     w_out = jnp.swapaxes(w_out, 1, 2)
     taps = jnp.swapaxes(taps, 0, 1)
     vm = pl.BlockSpec(memory_space=pltpu.VMEM)
+    anywhere = pl.BlockSpec(memory_space=pl.ANY)
     slots = (g.nz, g.ny, g.nc, 2, g.kr, g.ch)
     rows, ch = g.rows, g.ch
     most = max(g.ny, g.nz)
@@ -566,7 +566,7 @@
         pltpu.VMEM((g.nx, rows, ch), BF16),
         pltpu.VMEM((g.nx, rows, ch), BF16),
         pltpu.VMEM((g.nx, rows, ch), BF16),
-        pltpu.VMEM((g.nx, rows, ch), BF16),
+        pltpu.VMEM((rows, g.d), BF16),
         pltpu.VMEM((rows, ch), F32),
         pltpu.VMEM((rows, ch), F32),
         pltpu.VMEM((g.strips, HALO + rows, 128), F32),
@@ -585,6 +585,8 @@
         pltpu.VMEM((2, 2, rows, ch), BF16),
         pltpu.VMEM((3, rows, ch), F32),
         pltpu.VMEM((rows, ch), BF16),
+        pltpu.VMEM((g.taps, 2, ch), F32),
+        dma((8,)),
         dma((4, 2)),
         dma((4, 2)),
         dma((5, 2)),
@@ -605,7 +607,7 @@
     return pl.pallas_call(
         functools.partial(body, g),
         out_shape=jax.ShapeDtypeStruct((rows, ch), BF16),
-        in_specs=[vm] * 9,
+        in_specs=[anywhere, vm, anywhere, anywhere, anywhere, vm, vm, anywhere, vm],
         out_specs=vm,
         scratch_shapes=scratch,
         compiler_params=pltpu.CompilerParams(

time: 106 us -> 102 us (0.962)
  the two profiles are of different devices: /device:TPU:8 before, /device:TPU:2 now
where the time goes in v5:
time: 102 us
  Pallas kernels  100 us (98%)
  local copies, waits for them, and re-layouts  1.72 us (2%)
    pallas_call x1, Pallas kernels, local(): pl.pallas_call(functools.partial(body, g), out_shape=jax.ShapeDtypeStruct...  100 us

profile of v5, /device:TPU:2, one launch (start us, length us, event | category | flops | bytes accessed | tf_op | source)
XLA Modules:
  0.0 101.8 jit_solution(11975171826720806725)
XLA Ops:
  0.0 100.1 %shard_map.91 = bf16[320,512]{1,0:T(8,128)(2,1)} custom-call(bf16[320,512]{1,0:T(8,128)(2,1)} %tok.1, f32[2,2048]{1,0:T(2,128)} %pre_gain.1, bf16[2,16,512]{2,1,0:T(8,128)(2,1)} %wv.1, bf16[2,16,512]{2,1,0:T(8,128)(2,1)} %wg.1, f32[31,2,512]{2,1,0:T(2,128)} %bitcast.2, f32[2,512]{1,0:T(2,128)} %ngain.1, f32[2,512]{1,0:T(2,128)} %nshift.1, ...), custom_call_target="tpu_custom_call" | custom-call | tf_op jit(solution)/shard_map/pallas_call | solution.py:607
  100.1 1.7 %copy.11 = bf16[320,512]{1,0:T(8,128)(2,1)} copy(bf16[320,512]{1,0:T(8,128)(2,1)} %shard_map.91) | data formatting | bytes 655360

commit v6 on v5

--- a/solution.py
+++ b/solution.py
@@ -310,23 +310,25 @@
         lo, n, _ = g.chunks[q]
         loop(fn, lo // g.rb, (lo + n) // g.rb)
 
+    def lane_groups(v):
+        return sum(v[:, k * 128 : (k + 1) * 128] * v[:, k * 128 : (k + 1) * 128] for k in range(g.strips))
+
     def norm_rows(layer, i):
         rows = pl.ds(i * g.rb, g.rb)
         if layer == 1:
-            square = jnp.zeros((g.rb, 1), F32)
+            square = jnp.zeros((g.rb, 128), F32)
             for j in range(g.nx):
-                v = PJ[j, rows, :].astype(F32)
-                square += jnp.sum(v * v, -1, keepdims=True)
-            scale = lax.rsqrt(square / g.d + EPSILON)
-        total = jnp.zeros((g.rb, 1), F32)
+                square += lane_groups(PJ[j, rows, :].astype(F32))
+            scale = lax.rsqrt(jnp.sum(square, -1, keepdims=True) / g.d + EPSILON)
+        total = jnp.zeros((g.rb, 128), F32)
         for j in range(g.nx):
             v = X0[j, rows, :].astype(F32)
             if layer == 1:
                 v = v + PJ[j, rows, :].astype(F32) * scale * PG[j, 0:1, :]
                 X1[j, rows, :] = v.astype(BF16)
                 v = v.astype(BF16).astype(F32)
-            total += jnp.sum(v * v, -1, keepdims=True)
-        inv = lax.rsqrt(total / g.d + EPSILON)
+            total += lane_groups(v)
+        inv = lax.rsqrt(jnp.sum(total, -1, keepdims=True) / g.d + EPSILON)
         for j in range(g.nx):
             v = (X0, X1)[layer][j, rows, :].astype(F32)
             cols = pl.ds(j * g.ch, g.ch)
@@ -464,6 +466,7 @@
         over(q, combine)
 
     A, B = 0, 1
+    early = g.split // g.rb + 1
     for layer in range(2):
         if layer == 0:
             loop(lambda i: norm_rows(0, i), 0, g.blocks)
@@ -487,6 +490,7 @@
             project_in(1, rows_of(A))
             over(A, gate)
             fringe_send(1)
+            loop(lambda i: convolve(1, A, i), early, g.blocks)
             spread_end(1, B, PJ)
             over(B, lambda i: norm_rows(1, i))
             project_in(1, rows_of(B))
@@ -494,7 +498,7 @@
             finish(3)
         if layer == 0:
             loads[-1].wait()
-        over(A, lambda i: convolve(layer, A, i))
+        loop(lambda i: convolve(layer, A, i), early - 1, g.blocks if layer == 0 else early)
         stats_send(layer, A)
         loop(lambda i: convolve(layer, B, i), 1, g.split // g.rb)
         fringe_take(layer)

time: 102 us -> 102 us (level)
  the two profiles are of different devices: /device:TPU:2 before, /device:TPU:8 now
where the time goes in v6:
time: 102 us
  Pallas kernels  100 us (98%)
  local copies, waits for them, and re-layouts  1.72 us (2%)
    pallas_call x1, Pallas kernels, local(): pl.pallas_call(functools.partial(body, g), out_shape=jax.ShapeDtypeStruct...  100 us

profile of v6, /device:TPU:8, one launch (start us, length us, event | category | flops | bytes accessed | tf_op | source)
XLA Modules:
  0.0 101.7 jit_solution(15323405810204949527)
XLA Ops:
  0.0 100.0 %shard_map.91 = bf16[320,512]{1,0:T(8,128)(2,1)} custom-call(bf16[320,512]{1,0:T(8,128)(2,1)} %tok.1, f32[2,2048]{1,0:T(2,128)} %pre_gain.1, bf16[2,16,512]{2,1,0:T(8,128)(2,1)} %wv.1, bf16[2,16,512]{2,1,0:T(8,128)(2,1)} %wg.1, f32[31,2,512]{2,1,0:T(2,128)} %bitcast.2, f32[2,512]{1,0:T(2,128)} %ngain.1, f32[2,512]{1,0:T(2,128)} %nshift.1, ...), custom_call_target="tpu_custom_call" | custom-call | tf_op jit(solution)/shard_map/pallas_call | solution.py:611
  100.0 1.7 %copy.11 = bf16[320,512]{1,0:T(8,128)(2,1)} copy(bf16[320,512]{1,0:T(8,128)(2,1)} %shard_map.91) | data formatting | bytes 655360

commit v7 on v6

--- a/solution.py
+++ b/solution.py
@@ -514,12 +514,12 @@
         over(B, lambda i: activate(layer, B, i))
         shares(layer, B)
         relay_shares(layer, A)
+        own_share(layer, A)
+        relay_shares(layer, B)
+        own_share(layer, B)
         if layer == 0:
             advance(2, 1)
             advance(3, 1)
-        own_share(layer, A)
-        relay_shares(layer, B)
-        own_share(layer, B)
         for q in (A, B):
             shares_end(layer, q)
             if layer == 0:

time: 102 us -> 103 us (level)
  the two profiles are of different devices: /device:TPU:8 before, /device:TPU:2 now
where the time goes in v7:
time: 103 us; the launch traced here: 102 us
  Pallas kernels  101 us (98%)
  local copies, waits for them, and re-layouts  1.72 us (2%)
    pallas_call x1, Pallas kernels, local(): pl.pallas_call(functools.partial(body, g), out_shape=jax.ShapeDtypeStruct...  101 us

profile of v7, /device:TPU:2, one launch (start us, length us, event | category | flops | bytes accessed | tf_op | source)
XLA Modules:
  0.0 102.5 jit_solution(7353220962932083571)
XLA Ops:
  0.0 100.8 %shard_map.91 = bf16[320,512]{1,0:T(8,128)(2,1)} custom-call(bf16[320,512]{1,0:T(8,128)(2,1)} %tok.1, f32[2,2048]{1,0:T(2,128)} %pre_gain.1, bf16[2,16,512]{2,1,0:T(8,128)(2,1)} %wv.1, bf16[2,16,512]{2,1,0:T(8,128)(2,1)} %wg.1, f32[31,2,512]{2,1,0:T(2,128)} %bitcast.2, f32[2,512]{1,0:T(2,128)} %ngain.1, f32[2,512]{1,0:T(2,128)} %nshift.1, ...), custom_call_target="tpu_custom_call" | custom-call | tf_op jit(solution)/shard_map/pallas_call | solution.py:611
  100.8 1.7 %copy.11 = bf16[320,512]{1,0:T(8,128)(2,1)} copy(bf16[320,512]{1,0:T(8,128)(2,1)} %shard_map.91) | data formatting | bytes 655360
